TPU v7x, 32 devices: a whole 2x2x4 slice. The times are simulated.
32 devices in a mesh: kv: 16 (over z, x, core), tp: 2 (over y).
Axes of the slice: x: 2, y: 2, z: 4, core: 2. Of those that a mesh axis runs over, the one named last changes fastest.
Arguments:
- hidden_in: bfloat16 [4, 1024, 2048], P(None, 'kv'), may hold values from -84 to 84
- w_query: bfloat16 [2048, 1024], P(None, 'tp'), may hold values from -0.125 to 0.125
- w_cmp_key: bfloat16 [2048, 256], P(None, 'tp'), may hold values from -0.125 to 0.125
- w_cmp_value: bfloat16 [2048, 256], P(None, 'tp'), may hold values from -0.8838835 to 0.8838835
- w_sel_key: bfloat16 [2048, 256], P(None, 'tp'), may hold values from -0.125 to 0.125
- w_sel_value: bfloat16 [2048, 256], P(None, 'tp'), may hold values from -0.8838835 to 0.8838835
- w_gate: bfloat16 [2048, 2, 16], replicated, may hold values from -0.125 to 0.125
- cmp_key_in: bfloat16 [2048, 128], replicated, may hold values from -0.125 to 0.125
- cmp_key_out: bfloat16 [128, 64], replicated, may hold values from -0.5 to 0.5
- cmp_value_in: bfloat16 [2048, 128], replicated, may hold values from -0.125 to 0.125
- cmp_value_out: bfloat16 [128, 64], replicated, may hold values from -0.5 to 0.5
- out_gain: float32 [1024], replicated, may hold values from 0.1 to 1.9
- w_out: bfloat16 [1024, 2048], replicated, may hold values from -0.1875 to 0.1875
- seq_lengths: int32 [4], replicated, may hold values from 1 to 1024, 1638 in all
- chosen: int32 [4, 16, 4, 16], P(None, 'kv', 'tp'), may hold values from -1 to 15, as said below
Outputs:
- attended: bfloat16 [4, 1024, 2048], P(None, 'kv', 'tp')
Inputs may be any that keep to these rules, and one draw needn't show every extreme that they name: chosen[s, b, g, 0] is b itself. Every other entry is -1 or a block index below b, and the entries of one list that are not -1 are distinct. For each block index and key group, the entries after the first slot that name that index all lie in the lists of a single sequence.
All inputs are finite; a program needn't handle non-finite values.
Results may differ from a plain program's by a relative error of at most 0.012.
The roundings to bfloat16 on the way count: a program that leaves them out, or rounds other values in their place, can miss the bound.
Values may be sent and summed in bfloat16 or wider, within the bound.
A program may use at most 64 MiB of HBM per device.

v0:
```python
import functools
import math

import jax
import jax.numpy as jnp
from jax import lax
from jax.experimental import pallas as pl
from jax.experimental.pallas import tpu as pltpu
from jax.sharding import PartitionSpec as P

HEADS = 16
HEAD_DIM = 64
CMP_STRIDE = 16
CMP_BLOCK = 32
TOPK = 16


theta_base = 500000.0
norm_eps = 1e-06


def rotate(values, positions):
    width = values.shape[-1]
    half = width // 2
    inverse = jnp.exp(
        -jnp.log(jnp.float32(theta_base)) * jnp.arange(0, width, 2).astype(jnp.float32) / width
    )
    angle = positions.astype(jnp.float32)[:, None] * inverse[None, :]
    cosine = jnp.cos(angle)[:, None, :]
    sine = jnp.sin(angle)[:, None, :]
    first = values[..., :half]
    second = values[..., half:]
    return jnp.concatenate(
        [first * cosine - second * sine, second * cosine + first * sine], axis=-1
    )


def masked_weights(scores, valid):
    top = jnp.max(jnp.where(valid, scores, -1e30), axis=-1, keepdims=True)
    expd = jnp.where(valid, jnp.exp(scores - top), 0.0)
    total = jnp.sum(expd, axis=-1, keepdims=True)
    return (expd / jnp.maximum(total, 1.0)).astype(jnp.bfloat16)


def compress(raw, prior, weight_in, weight_out):
    seqs, span, groups, width = raw.shape
    extended = jnp.concatenate([prior, raw], axis=1)
    count = span // CMP_STRIDE
    front = extended[:, :span].reshape(seqs, count, CMP_STRIDE, groups, width)
    back = extended[:, CMP_STRIDE:].reshape(seqs, count, CMP_STRIDE, groups, width)
    window = jnp.concatenate([front, back], axis=2).transpose(0, 1, 3, 2, 4)
    window = window.reshape(seqs * count * groups, CMP_BLOCK * width)
    inner = jax.nn.gelu(jnp.dot(window, weight_in, preferred_element_type=jnp.float32)).astype(
        jnp.bfloat16
    )
    return jnp.dot(inner, weight_out, preferred_element_type=jnp.float32).reshape(
        seqs, count, groups, width
    )


def shards(
    hidden_in,
    w_query,
    w_cmp_key,
    w_cmp_value,
    w_sel_key,
    w_sel_value,
    w_gate,
    cmp_key_in,
    cmp_key_out,
    cmp_value_in,
    cmp_value_out,
    out_gain,
    w_out,
    seq_lengths,
    chosen,
):
    seqs, span, width = hidden_in.shape
    block_list = lax.axis_size("kv")
    place = lax.axis_index("kv")
    column = lax.axis_index("tp")
    local_heads = w_query.shape[1] // HEAD_DIM
    local_groups = w_sel_key.shape[1] // HEAD_DIM
    per_group = local_heads // local_groups
    count = span // CMP_STRIDE
    scale = HEAD_DIM ** (-0.5)
    rows = hidden_in.reshape(seqs * span, width)
    positions = place * span + jnp.arange(span, dtype=jnp.int32)

    def project(weight_matrix, heads):
        return jnp.dot(rows, weight_matrix, preferred_element_type=jnp.float32).reshape(
            seqs, span, heads, HEAD_DIM
        )

    queries = rotate(project(w_query, local_heads), positions).astype(jnp.bfloat16)
    sel_pairs = jnp.concatenate(
        [rotate(project(w_sel_key, local_groups), positions), project(w_sel_value, local_groups)],
        axis=-1,
    ).astype(jnp.bfloat16)
    raw_pairs = jnp.concatenate(
        [project(w_cmp_key, local_groups), project(w_cmp_value, local_groups)], axis=-1
    ).astype(jnp.bfloat16)
    prior = jnp.zeros((seqs, CMP_STRIDE, local_groups, HEAD_DIM), jnp.bfloat16)
    ends = place * span + jnp.arange(count, dtype=jnp.int32) * CMP_STRIDE + CMP_STRIDE - 1
    cmp_keys = rotate(compress(raw_pairs[..., :HEAD_DIM], prior, cmp_key_in, cmp_key_out), ends)
    cmp_values = compress(raw_pairs[..., HEAD_DIM:], prior, cmp_value_in, cmp_value_out)
    cmp_piece = jnp.concatenate(
        [cmp_keys.astype(jnp.bfloat16), cmp_values.astype(jnp.bfloat16)], axis=-1
    )[:, None]
    picks = chosen[:, 0]
    every_list = lax.all_gather(picks[None, :, :, 1:], "kv", axis=0, tiled=True)
    named = jnp.any(every_list == place, axis=(0, 3)).astype(jnp.int32)
    seq_ids = jnp.arange(seqs, dtype=jnp.int32)[:, None]
    exported_seq = jnp.sum(named * seq_ids, axis=0)
    selector = seq_ids == exported_seq[None, :]
    export = jnp.sum(
        jnp.where(selector[:, None, :, None], sel_pairs, jnp.zeros((), jnp.bfloat16)), axis=0
    )
    export = export[None]
    remote_pairs, remote_entries = (
        lax.all_gather(export, "kv", axis=0, tiled=True),
        lax.all_gather(cmp_piece, "kv", axis=1, tiled=True),
    )
    gate_all = jnp.dot(rows, w_gate.reshape(width, 2 * HEADS), preferred_element_type=jnp.float32)
    gate_all = gate_all.reshape(seqs, span, 2, HEADS)
    gates = jax.nn.sigmoid(lax.dynamic_slice_in_dim(gate_all, column * local_heads, local_heads, 3))
    entry = jnp.arange(block_list * count, dtype=jnp.int32)
    entry_end = entry * CMP_STRIDE + CMP_STRIDE - 1
    cmp_valid = ((entry >= 1)[None, :] & (entry_end[None, :] <= positions[:, None]))[None, None]
    key_pos = jnp.arange(span, dtype=jnp.int32)
    own_valid = key_pos[None, :] <= key_pos[:, None]

    def one_sequence(args):
        seq_queries, seq_entries, seq_picks, seq_pairs, seq_gates, seq_length = args
        block_q = seq_queries.reshape(span, local_groups, per_group, HEAD_DIM)
        entries = seq_entries.reshape(block_list * count, local_groups, 2 * HEAD_DIM)
        scores = (
            jnp.einsum(
                "qghd,egd->ghqe",
                block_q,
                entries[..., :HEAD_DIM],
                preferred_element_type=jnp.float32,
            )
            * scale
        )
        weights = masked_weights(scores, cmp_valid)
        cmp_out = jnp.einsum(
            "ghqe,egd->qghd", weights, entries[..., HEAD_DIM:], preferred_element_type=jnp.float32
        )
        far = jnp.maximum(seq_picks[:, 1:], 0)
        fetched = jax.vmap(lambda table, index: table[index], in_axes=(2, 0))(remote_pairs, far)
        near = jnp.transpose(seq_pairs, (1, 0, 2))[:, None]
        pairs = jnp.concatenate([near, fetched], axis=1).reshape(
            local_groups, TOPK * span, 2 * HEAD_DIM
        )
        far_live = jnp.broadcast_to(
            (seq_picks[:, 1:] >= 0)[:, None, :, None], (local_groups, span, TOPK - 1, span)
        )
        near_live = jnp.broadcast_to(own_valid[None, :, None, :], (local_groups, span, 1, span))
        sel_valid = jnp.concatenate([near_live, far_live], axis=2).reshape(
            local_groups, 1, span, TOPK * span
        )
        scores_s = (
            jnp.einsum(
                "qghd,gmd->ghqm", block_q, pairs[..., :HEAD_DIM], preferred_element_type=jnp.float32
            )
            * scale
        )
        weights_s = masked_weights(scores_s, sel_valid)
        sel_out = jnp.einsum(
            "ghqm,gmd->qghd", weights_s, pairs[..., HEAD_DIM:], preferred_element_type=jnp.float32
        )
        split = seq_gates.reshape(span, 2, local_groups, per_group, 1)
        mixed = split[:, 0] * cmp_out + split[:, 1] * sel_out
        mixed = jnp.where((positions < seq_length)[:, None, None, None], mixed, 0.0)
        return mixed.reshape(span, local_heads * HEAD_DIM).astype(jnp.bfloat16)

    mixed = lax.map(one_sequence, (queries, remote_entries, picks, sel_pairs, gates, seq_lengths))
    mixed = mixed.reshape(seqs * span, local_heads * HEAD_DIM)
    out_width = width // lax.axis_size("tp")
    own_columns = lax.dynamic_slice_in_dim(w_out, column * out_width, out_width, 1)
    piece_wide = lax.all_gather(mixed, "tp", axis=1, tiled=True).astype(jnp.float32)
    scaled_piece = (piece_wide * out_gain[None, :]).astype(jnp.bfloat16)
    total = jnp.dot(scaled_piece, own_columns, preferred_element_type=jnp.float32)
    squares = jnp.sum(piece_wide * piece_wide, axis=-1)
    row_scale = lax.rsqrt(squares / (HEADS * HEAD_DIM) + norm_eps)
    return (total * row_scale[:, None]).astype(jnp.bfloat16).reshape(seqs, span, out_width)


FAR = -1e30
PLANE = 4
VMEM_BYTES = 60 * 1024 * 1024
f32 = jnp.float32
bf16 = jnp.bfloat16


def dot(a, b):
    return jnp.dot(a, b, preferred_element_type=f32)


def dot_t(a, b):
    return lax.dot_general(a, b, (((1,), (1,)), ((), ())), preferred_element_type=f32)


def turn(values, cosine, sine):
    lane = lax.broadcasted_iota(jnp.int32, values.shape, 1)
    other = jnp.where(
        lane % HEAD_DIM < HEAD_DIM // 2,
        pltpu.roll(values, 128 - HEAD_DIM // 2, 1),
        pltpu.roll(values, HEAD_DIM // 2, 1),
    )
    return values * cosine + other * sine


def gelu(x):
    return 0.5 * x * (1.0 + jnp.tanh(0.7978845608028654 * (x + 0.044715 * (x * x * x))))


def layer_kernel(
    n, seqs, span, heads,
    lens_ref, picks_ref, gain_ref, kout_ref, vout_ref,
    rows_ref, wq_ref, wck_ref, wcv_ref, wsk_ref, wsv_ref, wg_ref, kin_ref, vin_ref, wout_ref,
    out_ref,
    rows, wq, ws, wg, kin, vin, weight,
    q_buf, sk_buf, sv_buf, raw, gate_buf, lists, blobs, own, other, bias, near, partial,
    load_sem, pick_send, pick_recv, blob_send, blob_recv, half_send, half_recv,
):
    me = lax.axis_index("kv")
    column = lax.axis_index("tp")
    planes = n // PLANE
    z, x, c = me // PLANE, (me // 2) % 2, me % 2
    depth = heads * HEAD_DIM
    wide = out_ref.shape[1]
    count = span // CMP_STRIDE
    entries = seqs * count
    half = heads // 2
    mesh_id = pl.DeviceIdType.MESH

    pairs = [(rows_ref, rows)]
    for i, ref in enumerate((wsk_ref, wsv_ref, wck_ref, wcv_ref)):
        pairs.append((ref, ws.at[:, i * 128 : (i + 1) * 128]))
    pairs += [(kin_ref, kin), (vin_ref, vin), (wq_ref, wq), (wg_ref, wg)]
    for i in range(2):
        side = column if i == 0 else 1 - column
        block = wout_ref.at[
            pl.ds(pl.multiple_of(side * depth, depth), depth),
            pl.ds(pl.multiple_of(column * wide, wide), wide),
        ]
        pairs.append((block, weight.at[i]))
    loads = [pltpu.make_async_copy(a, b, load_sem.at[i]) for i, (a, b) in enumerate(pairs)]
    for load in loads:
        load.start()

    barrier = pltpu.get_barrier_semaphore()
    for d in range(1, n):
        pl.semaphore_signal(
            barrier, inc=1, device_id={"kv": (me + d) % n}, device_id_type=mesh_id
        )
    pl.semaphore_signal(barrier, inc=1, device_id={"tp": 1 - column}, device_id_type=mesh_id)

    lane = lax.broadcasted_iota(jnp.int32, (span, 128), 1)
    low = lane < HEAD_DIM
    low_e = low[:entries]
    at = lax.broadcasted_iota(jnp.int32, (span, 128), 0)
    sign = jnp.where(lane % HEAD_DIM < HEAD_DIM // 2, -1.0, 1.0)
    power = (lane % (HEAD_DIM // 2) * 2).astype(f32)
    freq = jnp.exp(-math.log(theta_base) * power / HEAD_DIM)
    angle = (me * span + at).astype(f32) * freq
    cosine = jnp.cos(angle)
    sine = jnp.sin(angle) * sign
    end = me * span + (at[:entries] % count) * CMP_STRIDE + CMP_STRIDE - 1
    angle = end.astype(f32) * freq[:entries]
    cosine_e = jnp.cos(angle)
    sine_e = jnp.sin(angle) * sign[:entries]
    row_q = lax.broadcasted_iota(jnp.int32, (span, span), 0)
    near[...] = jnp.where(
        lax.broadcasted_iota(jnp.int32, (span, span), 1) <= row_q, 0.0, FAR
    )
    far_keys = n * span
    block = lax.broadcasted_iota(jnp.int32, (2, far_keys), 1) // span
    for s in range(seqs):
        listed = picks_ref[s]
        hit = jnp.zeros((2, far_keys), jnp.int32)
        for j in range(1, TOPK):
            hit = jnp.where(block == listed[:, j : j + 1], 1, hit)
        bias[s] = jnp.where(hit > 0, 0.0, FAR)

    pl.semaphore_wait(barrier, n)
    sent = []
    for d in range(1, n):
        copy = pltpu.make_async_remote_copy(
            src_ref=picks_ref, dst_ref=lists.at[me], send_sem=pick_send.at[d - 1],
            recv_sem=pick_recv.at[me], device_id={"kv": (me + d) % n}, device_id_type=mesh_id,
        )
        copy.start()
        sent.append(copy)

    for load in loads[:5]:
        load.wait()
    made = dot(rows[...], ws[...])
    for s in range(seqs):
        part = slice(s * span, (s + 1) * span)
        sk_buf[part, :] = turn(made[part, :128], cosine, sine).astype(bf16)
    sv_buf[...] = made[:, 128:256].astype(bf16)
    raw[0] = made[:, 256:384].astype(bf16).astype(f32)
    raw[1] = made[:, 384:512].astype(bf16).astype(f32)
    first = at[:entries] % count == 0
    mid = CMP_STRIDE * HEAD_DIM
    for branch, inner_weight, outer in ((0, kin, kout_ref), (1, vin, vout_ref)):
        loads[5 + branch].wait()
        left, right = [], []
        for j in range(0, CMP_STRIDE, 2):
            a = raw[branch, pl.ds(j, entries, stride=CMP_STRIDE), :]
            b = raw[branch, pl.ds(j + 1, entries, stride=CMP_STRIDE), :]
            left.append(jnp.where(low_e, a, pltpu.roll(b, HEAD_DIM, 1)))
            right.append(jnp.where(low_e, pltpu.roll(a, HEAD_DIM, 1), b))
        window = jnp.concatenate(
            [jnp.concatenate(left, axis=1), jnp.concatenate(right, axis=1)], axis=0
        ).astype(bf16)
        front = dot(window, inner_weight[:mid])
        back = dot(window, inner_weight[mid:])
        parts = []
        for g in range(2):
            shifted = pltpu.roll(front[g * entries : (g + 1) * entries], 1, 0)
            parts.append(back[g * entries : (g + 1) * entries] + jnp.where(first, 0.0, shifted))
        inner = gelu(jnp.concatenate(parts, axis=0)).astype(bf16)
        outer = jnp.concatenate([outer[...], outer[...]], axis=0)
        result = dot_t(inner, outer)
        result = jnp.where(low_e, result[:entries], result[entries:])
        if branch == 0:
            result = turn(result, cosine_e, sine_e)
        start = 2 * span + branch * entries
        blobs[me, start : start + entries, :] = result.astype(bf16)

    named = jnp.zeros((seqs, 2, TOPK), jnp.int32)
    for d in range(1, n):
        origin = (me + d) % n
        pltpu.make_async_remote_copy(
            src_ref=picks_ref, dst_ref=lists.at[origin], send_sem=pick_send.at[d - 1],
            recv_sem=pick_recv.at[origin], device_id={"kv": origin}, device_id_type=mesh_id,
        ).wait_recv()
        named = jnp.maximum(named, (lists[origin] == me).astype(jnp.int32))
    slot_at = lax.broadcasted_iota(jnp.int32, (seqs, 2, TOPK), 2)
    named = jnp.max(jnp.where(slot_at == 0, 0, named), axis=2, keepdims=True)
    key = jnp.zeros((span, 128), f32)
    value = jnp.zeros((span, 128), f32)
    for s in range(seqs):
        flag = jnp.where(low, named[s, 0:1, :], named[s, 1:2, :]) > 0
        key = jnp.where(flag, sk_buf[s * span : (s + 1) * span, :].astype(f32), key)
        value = jnp.where(flag, sv_buf[s * span : (s + 1) * span, :].astype(f32), value)
    blobs[me, 0:span, :] = key.astype(bf16)
    blobs[me, span : 2 * span, :] = value.astype(bf16)

    def pass_on(slot, dst, number):
        copy = pltpu.make_async_remote_copy(
            src_ref=blobs.at[slot], dst_ref=blobs.at[slot], send_sem=blob_send.at[number],
            recv_sem=blob_recv.at[slot], device_id={"kv": dst}, device_id_type=mesh_id,
        )
        copy.start()
        sent.append(copy)

    def arrived(slot):
        pltpu.make_async_remote_copy(
            src_ref=blobs.at[slot], dst_ref=blobs.at[slot], send_sem=blob_send.at[0],
            recv_sem=blob_recv.at[slot], device_id={"kv": (me + 1) % n}, device_id_type=mesh_id,
        ).wait_recv()

    across = z * PLANE + (1 - x) * 2 + c
    beside = z * PLANE + x * 2 + (1 - c)
    order = sorted(range(1, planes), key=lambda d: (min(d, planes - d), d))
    number = 0
    for d in order:
        pass_on(me, ((z + d) % planes) * PLANE + x * 2 + c, number)
        number += 1
    pass_on(me, across, number)
    pass_on(me, beside, number + 1)
    number += 2

    loads[7].wait()
    loads[8].wait()
    hidden = rows[...]
    for i in range(half):
        made = dot(hidden, wq[:, i * 128 : (i + 1) * 128])
        for s in range(seqs):
            v = turn(made[s * span : (s + 1) * span], cosine, sine) * (HEAD_DIM**-0.5)
            y = pltpu.roll(v, HEAD_DIM, 1)
            if 2 * i < half:
                even, odd = jnp.where(low, v, 0.0), jnp.where(low, y, 0.0)
            else:
                even, odd = jnp.where(low, 0.0, y), jnp.where(low, 0.0, v)
            base = (s * heads + 2 * i) * span
            q_buf[base : base + span, :] = even.astype(bf16)
            q_buf[base + span : base + 2 * span, :] = odd.astype(bf16)
    spread = 2 * wg_ref.shape[1]
    gate_buf[...] = jnp.zeros_like(gate_buf)
    gate_buf[:, :spread] = jax.nn.sigmoid(dot_t(hidden, wg[...].reshape(spread, rows.shape[1])))

    for d in order:
        slot = ((z + planes - d) % planes) * PLANE + x * 2 + c
        arrived(slot)
        pass_on(slot, across, number)
        pass_on(slot, beside, number + 1)
        number += 2
    for d in [0] + order:
        slot = ((z + planes - d) % planes) * PLANE + (1 - x) * 2 + c
        arrived(slot)
        pass_on(slot, beside, number)
        number += 1
    for d in [0] + order:
        origin = ((z + planes - d) % planes) * PLANE
        arrived(origin + x * 2 + (1 - c))
        arrived(origin + (1 - x) * 2 + (1 - c))

    slot = lax.broadcasted_iota(jnp.int32, (span, n * entries), 1)
    entry = (slot // entries) * count + slot % count
    entry_seq = (slot % entries) // count
    query_at = me * span + lax.broadcasted_iota(jnp.int32, (span, n * entries), 0)
    entry_ok = (entry >= 1) & (entry * CMP_STRIDE + CMP_STRIDE - 1 <= query_at)
    row_at = me * span + at
    far_k = blobs[:, 0:span, :].reshape(far_keys, 128)
    far_v = blobs[:, span : 2 * span, :].reshape(far_keys, 128)
    cmp_k = blobs[:, 2 * span : 2 * span + entries, :].reshape(n * entries, 128)
    cmp_v = blobs[:, 2 * span + entries :, :].reshape(n * entries, 128)

    def piece(s):
        return pltpu.make_async_remote_copy(
            src_ref=own.at[s], dst_ref=other.at[s], send_sem=half_send.at[s],
            recv_sem=half_recv.at[s], device_id={"tp": 1 - column}, device_id_type=mesh_id,
        )

    def one_sequence(s, carry):
        part = pl.ds(pl.multiple_of(s * span, span), span)
        near_k = sk_buf[part, :]
        near_v = sv_buf[part, :]
        gates = gate_buf[part, :]
        gates = jnp.where(column == 0, gates, pltpu.roll(gates, 128 - heads, 1))
        live = row_at < lens_ref[s]
        entry_bias = jnp.where(entry_ok & (entry_seq == s), 0.0, FAR)
        for g in range(2):
            start = pl.multiple_of((s * heads + g * half) * span, span)
            q = q_buf[pl.ds(start, half * span), :]
            sc = dot_t(q, cmp_k).reshape(half, span, n * entries) + entry_bias[None]
            top = jnp.maximum(jnp.max(sc, axis=-1, keepdims=True), -1e29)
            e = jnp.exp(sc - top)
            total = jnp.maximum(jnp.sum(e, axis=-1, keepdims=True), 1.0)
            w = (e * (1.0 / total)).astype(bf16).reshape(half * span, n * entries)
            cmp_out = dot(w, cmp_v)
            sf = dot_t(q, far_k) + bias[s, g : g + 1, :]
            sn = (dot_t(q, near_k).reshape(half, span, span) + near[...][None]).reshape(
                half * span, span
            )
            top = jnp.maximum(
                jnp.max(sf, axis=-1, keepdims=True), jnp.max(sn, axis=-1, keepdims=True)
            )
            ef = jnp.exp(sf - top)
            en = jnp.exp(sn - top)
            total = jnp.sum(ef, axis=-1, keepdims=True) + jnp.sum(en, axis=-1, keepdims=True)
            inverse = 1.0 / total
            sel_out = dot((ef * inverse).astype(bf16), far_v) + dot(
                (en * inverse).astype(bf16), near_v
            )
            mixed = []
            for h in range(half):
                span_h = slice(h * span, (h + 1) * span)
                head = g * half + h
                behind = spread // 2 + head
                mixed.append(
                    gates[:, head : head + 1] * cmp_out[span_h]
                    + gates[:, behind : behind + 1] * sel_out[span_h]
                )
            for h in range(0, half, 2):
                if g == 0:
                    pair = jnp.where(low, mixed[h], pltpu.roll(mixed[h + 1], HEAD_DIM, 1))
                else:
                    pair = jnp.where(low, pltpu.roll(mixed[h], HEAD_DIM, 1), mixed[h + 1])
                pair = jnp.where(live, pair, 0.0).astype(bf16)
                lanes = (g * half + h) * HEAD_DIM
                own[s, :, lanes : lanes + 128] = pair
        piece(s).start()
        return carry

    lax.fori_loop(0, seqs, one_sequence, 0)
    for load in loads[9:]:
        load.wait()
    gain_own = gain_ref[:, pl.ds(pl.multiple_of(column * depth, depth), depth)]
    gain_other = gain_ref[:, pl.ds(pl.multiple_of((1 - column) * depth, depth), depth)]

    def begin(s, carry):
        partial[s] = dot((own[s].astype(f32) * gain_own).astype(bf16), weight[0])
        return carry

    lax.fori_loop(0, seqs, begin, 0)

    def finish(s, carry):
        piece(s).wait_recv()
        a = own[s].astype(f32)
        b = other[s].astype(f32)
        squares = jnp.sum(a * a, axis=-1, keepdims=True) + jnp.sum(b * b, axis=-1, keepdims=True)
        row_scale = lax.rsqrt(squares / (2 * depth) + norm_eps)
        total = partial[s] + dot((b * gain_other).astype(bf16), weight[1])
        out_ref[pl.ds(pl.multiple_of(s * span, span), span), :] = (total * row_scale).astype(bf16)
        return carry

    lax.fori_loop(0, seqs, finish, 0)

    def close(s, carry):
        piece(s).wait_send()
        return carry

    lax.fori_loop(0, seqs, close, 0)
    for copy in sent:
        copy.wait_send()


def fused_shards(
    hidden_in,
    w_query,
    w_cmp_key,
    w_cmp_value,
    w_sel_key,
    w_sel_value,
    w_gate,
    cmp_key_in,
    cmp_key_out,
    cmp_value_in,
    cmp_value_out,
    out_gain,
    w_out,
    seq_lengths,
    chosen,
):
    seqs, span, width = hidden_in.shape
    n = lax.axis_size("kv")
    heads = w_query.shape[1] // HEAD_DIM
    total = seqs * span
    entries = total // CMP_STRIDE
    out_width = width // lax.axis_size("tp")
    small = w_sel_key.shape[1]
    vmem = pl.BlockSpec(memory_space=pltpu.VMEM)
    anywhere = pl.BlockSpec(memory_space=pl.ANY)
    gate_rows = jnp.transpose(w_gate, (1, 2, 0))
    out = pl.pallas_call(
        functools.partial(layer_kernel, n, seqs, span, heads),
        in_specs=[pl.BlockSpec(memory_space=pltpu.SMEM)] + [vmem] * 4 + [anywhere] * 10,
        out_specs=vmem,
        out_shape=jax.ShapeDtypeStruct((total, out_width), bf16),
        scratch_shapes=[
            pltpu.VMEM((total, width), bf16),
            pltpu.VMEM(w_query.shape, bf16),
            pltpu.VMEM((width, 4 * small), bf16),
            pltpu.VMEM(gate_rows.shape, bf16),
            pltpu.VMEM(cmp_key_in.shape, bf16),
            pltpu.VMEM(cmp_value_in.shape, bf16),
            pltpu.VMEM((2, heads * HEAD_DIM, out_width), bf16),
            pltpu.VMEM((heads * total, 128), bf16),
            pltpu.VMEM((total, small), bf16),
            pltpu.VMEM((total, small), bf16),
            pltpu.VMEM((2, total, small), f32),
            pltpu.VMEM((total, 128), f32),
            pltpu.VMEM((n, seqs, 2, TOPK), jnp.int32),
            pltpu.VMEM((n, 2 * span + 2 * entries, small), bf16),
            pltpu.VMEM((seqs, span, heads * HEAD_DIM), bf16),
            pltpu.VMEM((seqs, span, heads * HEAD_DIM), bf16),
            pltpu.VMEM((seqs, 2, n * span), f32),
            pltpu.VMEM((span, span), f32),
            pltpu.VMEM((seqs, span, out_width), f32),
            pltpu.SemaphoreType.DMA((11,)),
            pltpu.SemaphoreType.DMA((n,)),
            pltpu.SemaphoreType.DMA((n,)),
            pltpu.SemaphoreType.DMA((n,)),
            pltpu.SemaphoreType.DMA((n,)),
            pltpu.SemaphoreType.DMA((seqs,)),
            pltpu.SemaphoreType.DMA((seqs,)),
        ],
        compiler_params=pltpu.CompilerParams(
            collective_id=0, has_side_effects=True, vmem_limit_bytes=VMEM_BYTES
        ),
        name="layer",
    )(
        seq_lengths, chosen[:, 0], out_gain[None],
        jnp.transpose(cmp_key_out), jnp.transpose(cmp_value_out),
        hidden_in.reshape(total, width), w_query, w_cmp_key, w_cmp_value, w_sel_key,
        w_sel_value, gate_rows, cmp_key_in, cmp_value_in, w_out,
    )
    return out.reshape(seqs, span, out_width)


def fits(mesh):
    n = mesh.shape["kv"]
    return mesh.shape["tp"] == 2 and n % PLANE == 0 and n <= 32


def solution(mesh):
    placed = (
        P(None, "kv", None),
        P(None, "tp"),
        P(None, "tp"),
        P(None, "tp"),
        P(None, "tp"),
        P(None, "tp"),
        P(),
        P(),
        P(),
        P(),
        P(),
        P(),
        P(),
        P(),
        P(None, "kv", "tp", None),
    )
    return jax.shard_map(
        fused_shards if fits(mesh) else shards, mesh=mesh, in_specs=placed, out_specs=P(None, "kv", "tp"), check_vma=False
    )
```

profile of v0, /device:TPU:0, one launch (start us, length us, event | category | flops | bytes accessed | tf_op | source)
XLA Modules:
  0.0 37.2 jit_solution(1865367477580544888)
XLA Ops:
  0.0 35.4 %layer.1 = bf16[256,1024]{1,0:T(8,128)(2,1)} custom-call(s32[4]{0:T(128)} %lens_ref.1, s32[4,2,16]{2,1,0:T(2,128)} %bitcast.12, f32[1,1024]{1,0:T(1,128)} %bitcast.13, bf16[64,128]{1,0:T(8,128)(2,1)} %bitcast.10, bf16[64,128]{1,0:T(8,128)(2,1)} %bitcast.11, bf16[256,2048]{1,0:T(8,128)(2,1)} %bitcast.8, bf16[2048,512]{1,0:T(8,128)(2,1)} %wq_ref.1, ...), custom_call_target="tpu_custom_call" | custom-call | tf_op jit(solution)/shard_map/layer/pallas_call | solution.py:542
  35.4 1.9 %copy.17 = bf16[4,64,1024]{2,1,0:T(8,128)(2,1)} copy(bf16[4,64,1024]{2,1,0:T(8,128)(2,1)} %bitcast.7) | data formatting | bytes 1048576
where the time goes:
time: 37.5 us; the launch traced here: 37.2 us
  Pallas kernels  35.4 us (94%)
  local copies, waits for them, and re-layouts  1.87 us (5%)
    pallas_call x1, Pallas kernels, fused_shards(): pl.pallas_call(functools.partial(layer_kernel, n, seqs, span, heads), in_...  35.4 us
    unnamed x1, local copies, waits for them, and re-layouts  1.87 us

commit v1 on v0

--- a/solution.py
+++ b/solution.py
@@ -332,6 +332,25 @@
         start = 2 * span + branch * entries
         blobs[me, start : start + entries, :] = result.astype(bf16)
 
+    loads[7].wait()
+    loads[8].wait()
+    hidden = rows[...]
+    for i in range(half):
+        made = dot(hidden, wq[:, i * 128 : (i + 1) * 128])
+        for s in range(seqs):
+            v = turn(made[s * span : (s + 1) * span], cosine, sine) * (HEAD_DIM**-0.5)
+            y = pltpu.roll(v, HEAD_DIM, 1)
+            if 2 * i < half:
+                even, odd = jnp.where(low, v, 0.0), jnp.where(low, y, 0.0)
+            else:
+                even, odd = jnp.where(low, 0.0, y), jnp.where(low, 0.0, v)
+            base = (s * heads + 2 * i) * span
+            q_buf[base : base + span, :] = even.astype(bf16)
+            q_buf[base + span : base + 2 * span, :] = odd.astype(bf16)
+    spread = 2 * wg_ref.shape[1]
+    gate_buf[...] = jnp.zeros_like(gate_buf)
+    gate_buf[:, :spread] = jax.nn.sigmoid(dot_t(hidden, wg[...].reshape(spread, rows.shape[1])))
+
     named = jnp.zeros((seqs, 2, TOPK), jnp.int32)
     for d in range(1, n):
         origin = (me + d) % n
@@ -375,25 +394,6 @@
     pass_on(me, across, number)
     pass_on(me, beside, number + 1)
     number += 2
-
-    loads[7].wait()
-    loads[8].wait()
-    hidden = rows[...]
-    for i in range(half):
-        made = dot(hidden, wq[:, i * 128 : (i + 1) * 128])
-        for s in range(seqs):
-            v = turn(made[s * span : (s + 1) * span], cosine, sine) * (HEAD_DIM**-0.5)
-            y = pltpu.roll(v, HEAD_DIM, 1)
-            if 2 * i < half:
-                even, odd = jnp.where(low, v, 0.0), jnp.where(low, y, 0.0)
-            else:
-                even, odd = jnp.where(low, 0.0, y), jnp.where(low, 0.0, v)
-            base = (s * heads + 2 * i) * span
-            q_buf[base : base + span, :] = even.astype(bf16)
-            q_buf[base + span : base + 2 * span, :] = odd.astype(bf16)
-    spread = 2 * wg_ref.shape[1]
-    gate_buf[...] = jnp.zeros_like(gate_buf)
-    gate_buf[:, :spread] = jax.nn.sigmoid(dot_t(hidden, wg[...].reshape(spread, rows.shape[1])))
 
     for d in order:
         slot = ((z + planes - d) % planes) * PLANE + x * 2 + c
@@ -543,7 +543,7 @@
         functools.partial(layer_kernel, n, seqs, span, heads),
         in_specs=[pl.BlockSpec(memory_space=pltpu.SMEM)] + [vmem] * 4 + [anywhere] * 10,
         out_specs=vmem,
-        out_shape=jax.ShapeDtypeStruct((total, out_width), bf16),
+        out_shape=pltpu.VMEM((total, out_width), bf16),
         scratch_shapes=[
             pltpu.VMEM((total, width), bf16),
             pltpu.VMEM(w_query.shape, bf16),

time: 37.5 us -> 35.6 us (0.949)
  local copies, waits for them, and re-layouts: 1.87 us -> 0.8 us
  Pallas kernels: 35.4 us -> 34.6 us
    unnamed x1, local copies, waits for them, and re-layouts: 1.87 us -> 0.8 us
    pallas_call x1, Pallas kernels: 35.4 us -> 34.6 us  [fused_shards(): pl.pallas_call(functools.partial(layer_kernel, n, seqs, span, heads), in_...]
where the time goes in v1:
time: 35.6 us; the launch traced here: 35.4 us
  Pallas kernels  34.6 us (97%)
  local copies, waits for them, and re-layouts  0.8 us (2%)
    pallas_call x1, Pallas kernels, fused_shards(): pl.pallas_call(functools.partial(layer_kernel, n, seqs, span, heads), in_...  34.6 us
    unnamed x1, local copies, waits for them, and re-layouts  0.8 us

profile of v1, /device:TPU:0, one launch (start us, length us, event | category | flops | bytes accessed | tf_op | source)
XLA Modules:
  0.0 35.4 jit_solution(15520185113981448527)
XLA Ops:
  0.0 34.6 %layer.1 = bf16[256,1024]{1,0:T(8,128)(2,1)S(1)} custom-call(s32[4]{0:T(128)} %lens_ref.1, s32[4,2,16]{2,1,0:T(2,128)} %bitcast.12, f32[1,1024]{1,0:T(1,128)} %bitcast.13, bf16[64,128]{1,0:T(8,128)(2,1)} %bitcast.10, bf16[64,128]{1,0:T(8,128)(2,1)} %bitcast.11, bf16[256,2048]{1,0:T(8,128)(2,1)} %bitcast.8, bf16[2048,512]{1,0:T(8,128)(2,1)} %wq_ref.1, ...), custom_call_target="tpu_custom_call" | custom-call | tf_op jit(solution)/shard_map/layer/pallas_call | solution.py:542
  34.6 0.8 %copy.17 = bf16[4,64,1024]{2,1,0:T(8,128)(2,1)} copy(bf16[4,64,1024]{2,1,0:T(8,128)(2,1)S(1)} %bitcast.7) | data formatting | bytes 1048576

commit v2 on v1

v2 whole, which is shorter than its diff:
```python
import functools
import math

import jax
import jax.numpy as jnp
from jax import lax
from jax.experimental import pallas as pl
from jax.experimental.pallas import tpu as pltpu
from jax.sharding import PartitionSpec as P

HEADS = 16
HEAD_DIM = 64
CMP_STRIDE = 16
CMP_BLOCK = 32
TOPK = 16


theta_base = 500000.0
norm_eps = 1e-06


def rotate(values, positions):
    width = values.shape[-1]
    half = width // 2
    inverse = jnp.exp(
        -jnp.log(jnp.float32(theta_base)) * jnp.arange(0, width, 2).astype(jnp.float32) / width
    )
    angle = positions.astype(jnp.float32)[:, None] * inverse[None, :]
    cosine = jnp.cos(angle)[:, None, :]
    sine = jnp.sin(angle)[:, None, :]
    first = values[..., :half]
    second = values[..., half:]
    return jnp.concatenate(
        [first * cosine - second * sine, second * cosine + first * sine], axis=-1
    )


def masked_weights(scores, valid):
    top = jnp.max(jnp.where(valid, scores, -1e30), axis=-1, keepdims=True)
    expd = jnp.where(valid, jnp.exp(scores - top), 0.0)
    total = jnp.sum(expd, axis=-1, keepdims=True)
    return (expd / jnp.maximum(total, 1.0)).astype(jnp.bfloat16)


def compress(raw, prior, weight_in, weight_out):
    seqs, span, groups, width = raw.shape
    extended = jnp.concatenate([prior, raw], axis=1)
    count = span // CMP_STRIDE
    front = extended[:, :span].reshape(seqs, count, CMP_STRIDE, groups, width)
    back = extended[:, CMP_STRIDE:].reshape(seqs, count, CMP_STRIDE, groups, width)
    window = jnp.concatenate([front, back], axis=2).transpose(0, 1, 3, 2, 4)
    window = window.reshape(seqs * count * groups, CMP_BLOCK * width)
    inner = jax.nn.gelu(jnp.dot(window, weight_in, preferred_element_type=jnp.float32)).astype(
        jnp.bfloat16
    )
    return jnp.dot(inner, weight_out, preferred_element_type=jnp.float32).reshape(
        seqs, count, groups, width
    )


def shards(
    hidden_in,
    w_query,
    w_cmp_key,
    w_cmp_value,
    w_sel_key,
    w_sel_value,
    w_gate,
    cmp_key_in,
    cmp_key_out,
    cmp_value_in,
    cmp_value_out,
    out_gain,
    w_out,
    seq_lengths,
    chosen,
):
    seqs, span, width = hidden_in.shape
    block_list = lax.axis_size("kv")
    place = lax.axis_index("kv")
    column = lax.axis_index("tp")
    local_heads = w_query.shape[1] // HEAD_DIM
    local_groups = w_sel_key.shape[1] // HEAD_DIM
    per_group = local_heads // local_groups
    count = span // CMP_STRIDE
    scale = HEAD_DIM ** (-0.5)
    rows = hidden_in.reshape(seqs * span, width)
    positions = place * span + jnp.arange(span, dtype=jnp.int32)

    def project(weight_matrix, heads):
        return jnp.dot(rows, weight_matrix, preferred_element_type=jnp.float32).reshape(
            seqs, span, heads, HEAD_DIM
        )

    queries = rotate(project(w_query, local_heads), positions).astype(jnp.bfloat16)
    sel_pairs = jnp.concatenate(
        [rotate(project(w_sel_key, local_groups), positions), project(w_sel_value, local_groups)],
        axis=-1,
    ).astype(jnp.bfloat16)
    raw_pairs = jnp.concatenate(
        [project(w_cmp_key, local_groups), project(w_cmp_value, local_groups)], axis=-1
    ).astype(jnp.bfloat16)
    prior = jnp.zeros((seqs, CMP_STRIDE, local_groups, HEAD_DIM), jnp.bfloat16)
    ends = place * span + jnp.arange(count, dtype=jnp.int32) * CMP_STRIDE + CMP_STRIDE - 1
    cmp_keys = rotate(compress(raw_pairs[..., :HEAD_DIM], prior, cmp_key_in, cmp_key_out), ends)
    cmp_values = compress(raw_pairs[..., HEAD_DIM:], prior, cmp_value_in, cmp_value_out)
    cmp_piece = jnp.concatenate(
        [cmp_keys.astype(jnp.bfloat16), cmp_values.astype(jnp.bfloat16)], axis=-1
    )[:, None]
    picks = chosen[:, 0]
    every_list = lax.all_gather(picks[None, :, :, 1:], "kv", axis=0, tiled=True)
    named = jnp.any(every_list == place, axis=(0, 3)).astype(jnp.int32)
    seq_ids = jnp.arange(seqs, dtype=jnp.int32)[:, None]
    exported_seq = jnp.sum(named * seq_ids, axis=0)
    selector = seq_ids == exported_seq[None, :]
    export = jnp.sum(
        jnp.where(selector[:, None, :, None], sel_pairs, jnp.zeros((), jnp.bfloat16)), axis=0
    )
    export = export[None]
    remote_pairs, remote_entries = (
        lax.all_gather(export, "kv", axis=0, tiled=True),
        lax.all_gather(cmp_piece, "kv", axis=1, tiled=True),
    )
    gate_all = jnp.dot(rows, w_gate.reshape(width, 2 * HEADS), preferred_element_type=jnp.float32)
    gate_all = gate_all.reshape(seqs, span, 2, HEADS)
    gates = jax.nn.sigmoid(lax.dynamic_slice_in_dim(gate_all, column * local_heads, local_heads, 3))
    entry = jnp.arange(block_list * count, dtype=jnp.int32)
    entry_end = entry * CMP_STRIDE + CMP_STRIDE - 1
    cmp_valid = ((entry >= 1)[None, :] & (entry_end[None, :] <= positions[:, None]))[None, None]
    key_pos = jnp.arange(span, dtype=jnp.int32)
    own_valid = key_pos[None, :] <= key_pos[:, None]

    def one_sequence(args):
        seq_queries, seq_entries, seq_picks, seq_pairs, seq_gates, seq_length = args
        block_q = seq_queries.reshape(span, local_groups, per_group, HEAD_DIM)
        entries = seq_entries.reshape(block_list * count, local_groups, 2 * HEAD_DIM)
        scores = (
            jnp.einsum(
                "qghd,egd->ghqe",
                block_q,
                entries[..., :HEAD_DIM],
                preferred_element_type=jnp.float32,
            )
            * scale
        )
        weights = masked_weights(scores, cmp_valid)
        cmp_out = jnp.einsum(
            "ghqe,egd->qghd", weights, entries[..., HEAD_DIM:], preferred_element_type=jnp.float32
        )
        far = jnp.maximum(seq_picks[:, 1:], 0)
        fetched = jax.vmap(lambda table, index: table[index], in_axes=(2, 0))(remote_pairs, far)
        near = jnp.transpose(seq_pairs, (1, 0, 2))[:, None]
        pairs = jnp.concatenate([near, fetched], axis=1).reshape(
            local_groups, TOPK * span, 2 * HEAD_DIM
        )
        far_live = jnp.broadcast_to(
            (seq_picks[:, 1:] >= 0)[:, None, :, None], (local_groups, span, TOPK - 1, span)
        )
        near_live = jnp.broadcast_to(own_valid[None, :, None, :], (local_groups, span, 1, span))
        sel_valid = jnp.concatenate([near_live, far_live], axis=2).reshape(
            local_groups, 1, span, TOPK * span
        )
        scores_s = (
            jnp.einsum(
                "qghd,gmd->ghqm", block_q, pairs[..., :HEAD_DIM], preferred_element_type=jnp.float32
            )
            * scale
        )
        weights_s = masked_weights(scores_s, sel_valid)
        sel_out = jnp.einsum(
            "ghqm,gmd->qghd", weights_s, pairs[..., HEAD_DIM:], preferred_element_type=jnp.float32
        )
        split = seq_gates.reshape(span, 2, local_groups, per_group, 1)
        mixed = split[:, 0] * cmp_out + split[:, 1] * sel_out
        mixed = jnp.where((positions < seq_length)[:, None, None, None], mixed, 0.0)
        return mixed.reshape(span, local_heads * HEAD_DIM).astype(jnp.bfloat16)

    mixed = lax.map(one_sequence, (queries, remote_entries, picks, sel_pairs, gates, seq_lengths))
    mixed = mixed.reshape(seqs * span, local_heads * HEAD_DIM)
    out_width = width // lax.axis_size("tp")
    own_columns = lax.dynamic_slice_in_dim(w_out, column * out_width, out_width, 1)
    piece_wide = lax.all_gather(mixed, "tp", axis=1, tiled=True).astype(jnp.float32)
    scaled_piece = (piece_wide * out_gain[None, :]).astype(jnp.bfloat16)
    total = jnp.dot(scaled_piece, own_columns, preferred_element_type=jnp.float32)
    squares = jnp.sum(piece_wide * piece_wide, axis=-1)
    row_scale = lax.rsqrt(squares / (HEADS * HEAD_DIM) + norm_eps)
    return (total * row_scale[:, None]).astype(jnp.bfloat16).reshape(seqs, span, out_width)


FAR = -1e30
PLANE = 4
VMEM_BYTES = 60 * 1024 * 1024
f32 = jnp.float32
bf16 = jnp.bfloat16


def dot(a, b):
    return jnp.dot(a, b, preferred_element_type=f32)


def dot_t(a, b):
    return lax.dot_general(a, b, (((1,), (1,)), ((), ())), preferred_element_type=f32)


def swap(values):
    return pltpu.roll(values, HEAD_DIM, 1)


def turn(values, cosine, sine):
    lane = lax.broadcasted_iota(jnp.int32, values.shape, 1)
    other = jnp.where(
        lane % HEAD_DIM < HEAD_DIM // 2,
        pltpu.roll(values, 128 - HEAD_DIM // 2, 1),
        pltpu.roll(values, HEAD_DIM // 2, 1),
    )
    return values * cosine + other * sine


def gelu(x):
    return 0.5 * x * (1.0 + jnp.tanh(0.7978845608028654 * (x + 0.044715 * (x * x * x))))


def layer_kernel(
    n, seqs, span, heads,
    picks_ref, rows_ref, wsk_ref, wsv_ref, wck_ref, wcv_ref, kout_ref, vout_ref, kin_ref, vin_ref,
    wq_ref, wg_ref, lens_ref, gain_ref, wout_ref,
    out_ref,
    picks, rows, ws, kout, vout, kin, vin, wq, wg, lens, gain, weight,
    qn, sk_buf, svt, raw, gate_buf, hits, lists, ents, blobs, near_s, far_s, probs, vals,
    mix, own, other, partial,
    load_sem, pick_send, pick_recv, ent_send, ent_recv, blob_send, blob_recv, half_send, half_recv,
):
    me = lax.axis_index("kv")
    column = lax.axis_index("tp")
    planes = n // PLANE
    z, x, c = me // PLANE, (me // 2) % 2, me % 2
    depth = heads * HEAD_DIM
    wide = out_ref.shape[1]
    count = span // CMP_STRIDE
    entries = seqs * count
    half = heads // 2
    stack = seqs * HEAD_DIM
    across_q = half * span
    pairs = seqs // 2
    mesh_id = pl.DeviceIdType.MESH

    barrier = pltpu.get_barrier_semaphore()
    for d in range(1, n):
        pl.semaphore_signal(
            barrier, inc=1, device_id={"kv": (me + d) % n}, device_id_type=mesh_id
        )
    pl.semaphore_signal(barrier, inc=1, device_id={"tp": 1 - column}, device_id_type=mesh_id)

    jobs = [(picks_ref, picks), (rows_ref, rows)]
    for i, ref in enumerate((wsk_ref, wsv_ref, wck_ref, wcv_ref)):
        jobs.append((ref, ws.at[:, i * 128 : (i + 1) * 128]))
    jobs += [(kout_ref, kout), (vout_ref, vout), (kin_ref, kin), (vin_ref, vin)]
    jobs += [(wq_ref, wq), (wg_ref, wg), (lens_ref, lens), (gain_ref, gain)]
    for i in range(2):
        side = column if i == 0 else 1 - column
        block = wout_ref.at[
            pl.ds(pl.multiple_of(side * depth, depth), depth),
            pl.ds(pl.multiple_of(column * wide, wide), wide),
        ]
        jobs.append((block, weight.at[i]))
    loads = [pltpu.make_async_copy(a, b, load_sem.at[i]) for i, (a, b) in enumerate(jobs)]
    for load in loads:
        load.start()

    lane = lax.broadcasted_iota(jnp.int32, (span, 128), 1)
    low = lane < HEAD_DIM
    low_e = low[:entries]
    low_row = low[:1]
    at = lax.broadcasted_iota(jnp.int32, (span, 128), 0)
    sign = jnp.where(lane % HEAD_DIM < HEAD_DIM // 2, -1.0, 1.0)
    power = (lane % (HEAD_DIM // 2) * 2).astype(f32)
    freq = jnp.exp(-math.log(theta_base) * power / HEAD_DIM)
    angle = (me * span + at).astype(f32) * freq
    cosine = jnp.cos(angle)
    sine = jnp.sin(angle) * sign
    end = me * span + (at[:entries] % count) * CMP_STRIDE + CMP_STRIDE - 1
    angle = end.astype(f32) * freq[:entries]
    cosine_e = jnp.cos(angle)
    sine_e = jnp.sin(angle) * sign[:entries]

    for plane in range(1, planes):
        @pl.when(plane > z)
        def _():
            for g in range(2):
                for i in range(PLANE):
                    blobs[g, plane * PLANE + i] = jnp.zeros((span, 128), bf16)

    for d in range(1, n):
        @pl.when(d > me)
        def _():
            ents[d] = jnp.zeros((2 * entries, 128), bf16)

    loads[0].wait()
    slot_at = lax.broadcasted_iota(jnp.int32, (2 * seqs, TOPK), 1)
    listed = jnp.where(slot_at == 0, -1, picks[...])
    for b in range(n):
        hit = jnp.max(jnp.where(listed == b, 1.0, 0.0), axis=1, keepdims=True)
        hits[b] = jnp.broadcast_to(hit, (2 * seqs, 128))

    pl.semaphore_wait(barrier, n)
    sent = []

    def send(src, dst, ssem, rsem, target, when=None):
        copy = pltpu.make_async_remote_copy(
            src_ref=src, dst_ref=dst, send_sem=ssem, recv_sem=rsem,
            device_id=target, device_id_type=mesh_id,
        )
        if when is None:
            copy.start()
        else:
            pl.when(when)(copy.start)
        sent.append((copy, when))

    for d in range(1, n):
        send(picks, lists.at[me], pick_send.at[d - 1], pick_recv.at[me], {"kv": (me + d) % n})

    for load in loads[1:6]:
        load.wait()
    made = dot(rows[...], ws[...])
    sv = []
    for s in range(seqs):
        part = slice(s * span, (s + 1) * span)
        sk_buf[part, :] = turn(made[part, :128], cosine, sine).astype(bf16)
    svt[...] = jnp.transpose(made[:, 128:256]).astype(bf16)
    raw[0] = made[:, 256:384].astype(bf16).astype(f32)
    raw[1] = made[:, 384:512].astype(bf16).astype(f32)
    first = at[:entries] % count == 0
    mid = CMP_STRIDE * HEAD_DIM
    results = []
    for load in loads[6:10]:
        load.wait()
    for branch, inner_weight, outer in ((0, kin, kout), (1, vin, vout)):
        left, right = [], []
        for j in range(0, CMP_STRIDE, 2):
            a = raw[branch, pl.ds(j, entries, stride=CMP_STRIDE), :]
            b = raw[branch, pl.ds(j + 1, entries, stride=CMP_STRIDE), :]
            left.append(jnp.where(low_e, a, swap(b)))
            right.append(jnp.where(low_e, swap(a), b))
        window = jnp.concatenate(
            [jnp.concatenate(left, axis=1), jnp.concatenate(right, axis=1)], axis=0
        ).astype(bf16)
        front = dot(window, inner_weight[:mid])
        back = dot(window, inner_weight[mid:])
        parts = []
        for g in range(2):
            shifted = pltpu.roll(front[g * entries : (g + 1) * entries], 1, 0)
            parts.append(back[g * entries : (g + 1) * entries] + jnp.where(first, 0.0, shifted))
        inner = gelu(jnp.concatenate(parts, axis=0)).astype(bf16)
        results.append(dot_t(inner, jnp.concatenate([outer[...], outer[...]], axis=0)))
    for g in range(2):
        part = slice(g * entries, (g + 1) * entries)
        key = turn(results[0][part], cosine_e, sine_e)
        ents[me, part, :] = jnp.where(low_e, key, results[1][part]).astype(bf16)
    for d in range(1, n):
        send(
            ents.at[me], ents.at[me], ent_send.at[d - 1], ent_recv.at[me],
            {"kv": (me + d) % n}, me + d < n,
        )

    for load in loads[10:14]:
        load.wait()
    hidden = rows[...]
    for i in range(half):
        made = dot(hidden, wq[:, i * 128 : (i + 1) * 128])
        g, h = (2 * i) // half, (2 * i) % half
        turned = [
            turn(made[s * span : (s + 1) * span], cosine, sine) * (HEAD_DIM**-0.5)
            for s in range(seqs)
        ]
        for p in range(pairs):
            a, b = turned[2 * p], turned[2 * p + 1]
            even, odd = jnp.where(low, a, swap(b)), jnp.where(low, swap(a), b)
            lanes = slice(p * 128, (p + 1) * 128)
            qn[g, h * span : (h + 1) * span, lanes] = even.astype(bf16)
            qn[g, (h + 1) * span : (h + 2) * span, lanes] = odd.astype(bf16)
    spread = 2 * wg_ref.shape[1]
    logits = dot_t(wg[...].reshape(spread, rows.shape[1]), hidden)
    wide_at = lax.broadcasted_iota(jnp.int32, (1, seqs * span), 1)
    limit = jnp.zeros((1, seqs * span), jnp.int32)
    for s in range(seqs):
        limit = jnp.where(wide_at // span == s, lens[:, s : s + 1], limit)
    live = me * span + wide_at % span < limit
    for branch in range(2):
        base = branch * (spread // 2)
        mine = jnp.where(
            column == 0, logits[base : base + heads], logits[base + heads : base + 2 * heads]
        )
        mine = jnp.where(live, jax.nn.sigmoid(mine), 0.0)
        turned = [mine[:, p * 128 : (p + 1) * 128] for p in range(pairs)]
        swapped = [swap(t) for t in turned]
        for g in range(2):
            for s in range(seqs):
                for j in range(half // 2):
                    one = slice(g * half + 2 * j, g * half + 2 * j + 1)
                    two = slice(g * half + 2 * j + 1, g * half + 2 * j + 2)
                    t, w = turned[s // 2], swapped[s // 2]
                    if s % 2 == 0:
                        row = jnp.where(low_row, t[one], w[two])
                    else:
                        row = jnp.where(low_row, w[one], t[two])
                    number = (branch * 2 + g) * seqs + s
                    gate_buf[number : number + 1, j * 128 : (j + 1) * 128] = row

    named = jnp.zeros((2 * seqs, TOPK), f32)
    for d in range(1, n):
        origin = (me + d) % n
        pltpu.make_async_remote_copy(
            src_ref=picks, dst_ref=lists.at[origin], send_sem=pick_send.at[d - 1],
            recv_sem=pick_recv.at[origin], device_id={"kv": origin}, device_id_type=mesh_id,
        ).wait_recv()
        named = jnp.where(lists[origin] == me, 1.0, named)
    named = jnp.max(jnp.where(slot_at == 0, 0.0, named), axis=1, keepdims=True)
    named = jnp.broadcast_to(named, (2 * seqs, 128))
    key = jnp.zeros((span, 128), f32)
    for s in range(seqs):
        flag = jnp.where(low_row, named[2 * s : 2 * s + 1], named[2 * s + 1 : 2 * s + 2])
        key = key + flag * sk_buf[s * span : (s + 1) * span, :].astype(f32)
    for g in range(2):
        value = jnp.zeros((HEAD_DIM, 128), f32)
        for p in range(pairs):
            r0, r1 = 4 * p + g, 4 * p + 2 + g
            flag = jnp.where(low_row, named[r0 : r0 + 1], named[r1 : r1 + 1])
            block = svt[g * HEAD_DIM : (g + 1) * HEAD_DIM, p * 128 : (p + 1) * 128]
            value = value + flag * block.astype(f32)
        value = value + swap(value)
        blobs[g, me] = jnp.where(low, key if g == 0 else swap(key), value).astype(bf16)

    number = [0]

    def pass_on(g, slot, dst, when=None):
        ref = blobs.at[g, slot]
        send(ref, ref, blob_send.at[number[0]], blob_recv.at[g, slot], {"kv": dst}, when)
        number[0] += 1

    def arrived(g, slot):
        ref = blobs.at[g, slot]
        pltpu.make_async_remote_copy(
            src_ref=ref, dst_ref=ref, send_sem=blob_send.at[0],
            recv_sem=blob_recv.at[g, slot], device_id={"kv": (me + 1) % n}, device_id_type=mesh_id,
        ).wait_recv()

    across = z * PLANE + (1 - x) * 2 + c
    beside = z * PLANE + x * 2 + (1 - c)
    side_slot = x * 2 + c
    across_slot = (1 - x) * 2 + c
    for g in range(2):
        for d in range(planes - 1, 0, -1):
            pass_on(g, me, me + d * PLANE, z + d < planes)
        pass_on(g, me, across)
        pass_on(g, me, beside)

    def from_below(g, d):
        slot = jnp.maximum(z - d, 0) * PLANE + side_slot
        pl.when(z >= d)(lambda: arrived(g, slot))
        pass_on(g, slot, across, z >= d)
        pass_on(g, slot, beside, z >= d)

    def from_across(g, d):
        slot = jnp.maximum(z - d, 0) * PLANE + across_slot
        if d == 0:
            arrived(g, slot)
            pass_on(g, slot, beside)
        else:
            pl.when(z >= d)(lambda: arrived(g, slot))
            pass_on(g, slot, beside, z >= d)

    def from_beside(g):
        for d in range(planes):
            for column_x in (x, 1 - x):
                slot = jnp.maximum(z - d, 0) * PLANE + column_x * 2 + (1 - c)
                if d == 0:
                    arrived(g, slot)
                else:
                    pl.when(z >= d)(functools.partial(arrived, g, slot))

    key_at = lax.broadcasted_iota(jnp.int32, (span, across_q), 0)
    query_at = lax.broadcasted_iota(jnp.int32, (span, across_q), 1) % span
    near_bias = jnp.where(key_at <= query_at, 0.0, FAR)
    seq_lane = lax.broadcasted_iota(jnp.int32, (HEAD_DIM, seqs * span), 1) // span
    ones_at = lax.broadcasted_iota(jnp.int32, (16, seqs * span), 0)
    ones_lane = lax.broadcasted_iota(jnp.int32, (16, seqs * span), 1) // span
    near_keys = seqs * span
    near_top = {}

    def near_part(g):
        for s in range(seqs):
            block = sk_buf[s * span : (s + 1) * span, :].astype(f32)
            if g != s % 2:
                block = swap(block)
            block = jnp.where(low if s % 2 == 0 else ~low, block, 0.0).astype(bf16)
            lanes = slice((s // 2) * 128, (s // 2 + 1) * 128)
            score = dot_t(block, qn[g, :, lanes]) + near_bias
            near_s[g, s * span : (s + 1) * span, :] = score
            near_top[g, s] = jnp.max(score.reshape(span // 8, 8, across_q), axis=0)
            value = svt[g * HEAD_DIM : (g + 1) * HEAD_DIM, :].astype(f32)
            vals[g, s * HEAD_DIM : (s + 1) * HEAD_DIM, 0:near_keys] = jnp.where(
                seq_lane == s, value, 0.0
            ).astype(bf16)
        vals[g, stack : stack + 16, 0:near_keys] = jnp.where(
            ones_at == ones_lane, 1.0, 0.0
        ).astype(bf16)

    slots = n * entries
    entry_row = lax.broadcasted_iota(jnp.int32, (slots, 128), 0)
    entry_half = lax.broadcasted_iota(jnp.int32, (slots, 128), 1) // HEAD_DIM
    entry_seq = (entry_row % entries) // count
    slot_row = lax.broadcasted_iota(jnp.int32, (slots, across_q), 0)
    slot_query = lax.broadcasted_iota(jnp.int32, (slots, across_q), 1) % span
    slot_entry = (slot_row // entries) * count + slot_row % count
    entry_ok = (slot_entry >= 1) & (
        slot_entry * CMP_STRIDE + CMP_STRIDE - 1 <= me * span + slot_query
    )
    entry_bias = jnp.where(entry_ok, 0.0, FAR)
    value_lane = (lax.broadcasted_iota(jnp.int32, (HEAD_DIM, slots), 1) % entries) // count
    total_row = lax.broadcasted_iota(jnp.int32, (16, slots), 0)
    total_lane = (lax.broadcasted_iota(jnp.int32, (16, slots), 1) % entries) // count
    group_row = lax.broadcasted_iota(jnp.int32, (entries, across_q), 0)

    def wait_entries():
        for b in range(n):
            @pl.when(b < me)
            def _():
                pltpu.make_async_remote_copy(
                    src_ref=ents.at[b], dst_ref=ents.at[b], send_sem=ent_send.at[0],
                    recv_sem=ent_recv.at[b], device_id={"kv": (me + 1) % n},
                    device_id_type=mesh_id,
                ).wait_recv()

    def cmp_part(g):
        part = slice(g * entries, (g + 1) * entries)
        both = ents[:, part, :].reshape(slots, 128).astype(f32)
        twice = jnp.where(entry_half == 0, both, swap(both))
        keys = jnp.concatenate(
            [jnp.where(entry_seq == 2 * p + entry_half, twice, 0.0) for p in range(pairs)], axis=1
        ).astype(bf16)
        score = (dot_t(keys, qn[g]) + entry_bias).reshape(n, entries, across_q)
        top = jnp.max(score, axis=0)
        for step in (1, 2):
            top = jnp.maximum(
                top,
                jnp.where(
                    (group_row // step) % 2 == 0,
                    pltpu.roll(top, entries - step, 0),
                    pltpu.roll(top, step, 0),
                ),
            )
        top = jnp.maximum(top, -1e29)
        w = jnp.exp(score - top[None]).reshape(slots, across_q).astype(bf16)
        value = jnp.transpose(both)[HEAD_DIM:]
        left = [jnp.where(value_lane == s, value, 0.0) for s in range(seqs)]
        left.append(jnp.where(total_row == total_lane, 1.0, 0.0))
        made = dot(jnp.concatenate(left, axis=0).astype(bf16), w)
        for s in range(seqs):
            total = jnp.maximum(made[stack + s : stack + s + 1], 1.0)
            row = g * seqs + s
            factor = gate_buf[row : row + 1, :] / total
            block = slice(s * HEAD_DIM, (s + 1) * HEAD_DIM)
            mix[g, block, :] = made[block] * factor

    def far_part(g):
        tops = []
        for plane in range(planes):
            left = []
            for i in range(PLANE):
                b = plane * PLANE + i
                block = blobs[g, b].astype(f32)
                turned = swap(block)
                twice = jnp.where(low, block, turned)
                tiles = []
                for p in range(pairs):
                    r0, r1 = 4 * p + g, 4 * p + 2 + g
                    flag = jnp.where(low_row, hits[b, r0 : r0 + 1], hits[b, r1 : r1 + 1])
                    tiles.append(twice * flag)
                left.append(jnp.concatenate(tiles, axis=1))
                if i % 2 == 0:
                    before = turned
                else:
                    value = jnp.where(low, before, block)
                    lanes = slice(near_keys + (b - 1) * span, near_keys + (b + 1) * span)
                    for s in range(seqs):
                        r = 2 * s + g
                        flag = jnp.where(low_row, hits[b - 1, r : r + 1], hits[b, r : r + 1])
                        vals[g, s * HEAD_DIM : (s + 1) * HEAD_DIM, lanes] = (value * flag).astype(
                            bf16
                        )
                    flags = [
                        jnp.where(low_row, hits[b - 1, r : r + 1], hits[b, r : r + 1])
                        for r in range(g, 2 * seqs, 2)
                    ]
                    flags.append(jnp.zeros((16 - seqs, 128), f32))
                    vals[g, stack : stack + 16, lanes] = jnp.concatenate(flags, axis=0).astype(bf16)
            score = dot_t(jnp.concatenate(left, axis=0).astype(bf16), qn[g])
            far_s[plane * PLANE * span : (plane + 1) * PLANE * span, :] = score
            for i in range(PLANE):
                block = score[i * span : (i + 1) * span].reshape(span // 8, 8, across_q)
                tops.append(jnp.max(block, axis=0))
        wide_hits = [jnp.concatenate([hits[b], hits[b]], axis=1) for b in range(n)]
        refs = [jnp.full((1, across_q), 1e30, f32) for _ in range(n)]
        for s in range(seqs):
            r = 2 * s + g
            top = near_top[g, s]
            for b in range(n):
                top = jnp.maximum(top, jnp.where(wide_hits[b][r : r + 1] > 0, tops[b], FAR))
            top = jnp.max(top, axis=0, keepdims=True)
            for b in range(n):
                refs[b] = jnp.where(wide_hits[b][r : r + 1] > 0, top, refs[b])
            part = slice(s * span, (s + 1) * span)
            probs[part, :] = jnp.exp(near_s[g, part, :] - top).astype(bf16)
        for b in range(n):
            part = slice(b * span, (b + 1) * span)
            block = jnp.exp(far_s[part, :] - refs[b]).astype(bf16)
            probs[near_keys + b * span : near_keys + (b + 1) * span, :] = block
        made = dot(vals[g], probs[...])
        for p in range(pairs):
            tiles = []
            for s in (2 * p, 2 * p + 1):
                row = (2 + g) * seqs + s
                total = jnp.maximum(made[stack + s : stack + s + 1], 1.0)
                factor = gate_buf[row : row + 1, :] / total
                block = slice(s * HEAD_DIM, (s + 1) * HEAD_DIM)
                tiles.append(mix[g, block, :] + made[block] * factor)
            both = jnp.concatenate(tiles, axis=0)
            for j in range(half // 2):
                lanes = slice(j * 128, (j + 1) * 128)
                flipped = jnp.transpose(both[:, lanes])
                a, b = flipped[:span], flipped[span:]
                part = slice(2 * p * span, (2 * p + 1) * span)
                own[g, part, lanes] = jnp.where(low, a, swap(b)).astype(bf16)
                part = slice((2 * p + 1) * span, (2 * p + 2) * span)
                own[g, part, lanes] = jnp.where(low, swap(a), b).astype(bf16)
            for s in (2 * p, 2 * p + 1):
                piece(g, s).start()

    def piece(g, s):
        part = pl.ds(s * span, span)
        return pltpu.make_async_remote_copy(
            src_ref=own.at[g, part], dst_ref=other.at[g, part], send_sem=half_send.at[g, s],
            recv_sem=half_recv.at[g, s], device_id={"tp": 1 - column}, device_id_type=mesh_id,
        )

    for g in range(2):
        near_part(g)
    from_across(0, 0)
    if planes > 1:
        from_below(0, 1)
    from_across(1, 0)
    for d in range(2, planes):
        from_below(0, d)
        from_below(1, d - 1)
    wait_entries()
    cmp_part(0)
    for d in range(1, planes):
        from_across(0, d)
        if d == planes - 2:
            from_below(1, planes - 1)
    for d in range(1, planes - 1):
        from_across(1, d)
    if planes == 2:
        from_below(1, 1)
    from_beside(0)
    far_part(0)
    from_across(1, planes - 1)
    for load in loads[14:]:
        load.wait()
    cmp_part(1)
    from_beside(1)
    far_part(1)

    squares = jnp.zeros((seqs * span, 1), f32)
    total = jnp.zeros((seqs * span, wide), f32)
    group = half * HEAD_DIM

    def gains(side, g):
        return gain[:, pl.ds(pl.multiple_of(side * depth + g * group, group), group)]

    for g in range(2):
        a = own[g].astype(f32)
        squares = squares + jnp.sum(a * a, axis=1, keepdims=True)
        scaled = (a * gains(column, g)).astype(bf16)
        total = total + dot(scaled, weight[0, g * group : (g + 1) * group, :])
    for s in range(seqs):
        piece(0, s).wait_recv()
    a = other[0].astype(f32)
    squares = squares + jnp.sum(a * a, axis=1, keepdims=True)
    scaled = (a * gains(1 - column, 0)).astype(bf16)
    partial[...] = total + dot(scaled, weight[1, :group, :])
    for s in range(seqs):
        piece(1, s).wait_recv()
        part = slice(s * span, (s + 1) * span)
        a = other[1, part, :].astype(f32)
        square = squares[part] + jnp.sum(a * a, axis=1, keepdims=True)
        row_scale = lax.rsqrt(square / (2 * depth) + norm_eps)
        scaled = (a * gains(1 - column, 1)).astype(bf16)
        done = partial[part, :] + dot(scaled, weight[1, group:, :])
        out_ref[part, :] = (done * row_scale).astype(bf16)

    for g in range(2):
        for s in range(seqs):
            piece(g, s).wait_send()
    for copy, when in sent:
        if when is None:
            copy.wait_send()
        else:
            pl.when(when)(copy.wait_send)


def fused_shards(
    hidden_in,
    w_query,
    w_cmp_key,
    w_cmp_value,
    w_sel_key,
    w_sel_value,
    w_gate,
    cmp_key_in,
    cmp_key_out,
    cmp_value_in,
    cmp_value_out,
    out_gain,
    w_out,
    seq_lengths,
    chosen,
):
    seqs, span, width = hidden_in.shape
    n = lax.axis_size("kv")
    heads = w_query.shape[1] // HEAD_DIM
    total = seqs * span
    entries = total // CMP_STRIDE
    out_width = width // lax.axis_size("tp")
    small = w_sel_key.shape[1]
    half = heads // 2
    stack = seqs * HEAD_DIM
    across_q = half * span
    planes = n // PLANE
    anywhere = pl.BlockSpec(memory_space=pl.ANY)
    gate_rows = jnp.transpose(w_gate, (1, 2, 0))
    picks = chosen[:, 0].reshape(2 * seqs, TOPK)
    key_out, value_out = jnp.transpose(cmp_key_out), jnp.transpose(cmp_value_out)
    lens = seq_lengths[None]
    gain = out_gain[None]
    blob_sends = 2 * (planes + 1) + 2 * (2 * (planes - 1) + planes)
    out = pl.pallas_call(
        functools.partial(layer_kernel, n, seqs, span, heads),
        in_specs=[anywhere] * 15,
        out_specs=pl.BlockSpec(memory_space=pltpu.VMEM),
        out_shape=pltpu.VMEM((total, out_width), bf16),
        scratch_shapes=[
            pltpu.VMEM(picks.shape, jnp.int32),
            pltpu.VMEM((total, width), bf16),
            pltpu.VMEM((width, 4 * small), bf16),
            pltpu.VMEM(key_out.shape, bf16),
            pltpu.VMEM(value_out.shape, bf16),
            pltpu.VMEM(cmp_key_in.shape, bf16),
            pltpu.VMEM(cmp_value_in.shape, bf16),
            pltpu.VMEM(w_query.shape, bf16),
            pltpu.VMEM(gate_rows.shape, bf16),
            pltpu.VMEM(lens.shape, jnp.int32),
            pltpu.VMEM(gain.shape, f32),
            pltpu.VMEM((2, heads * HEAD_DIM, out_width), bf16),
            pltpu.VMEM((2, across_q, stack), bf16),
            pltpu.VMEM((total, small), bf16),
            pltpu.VMEM((small, total), bf16),
            pltpu.VMEM((2, total, small), f32),
            pltpu.VMEM((4 * seqs, across_q), f32),
            pltpu.VMEM((n, 2 * seqs, 128), f32),
            pltpu.VMEM((n,) + picks.shape, jnp.int32),
            pltpu.VMEM((n, 2 * entries, 128), bf16),
            pltpu.VMEM((2, n, span, 128), bf16),
            pltpu.VMEM((2, total, across_q), f32),
            pltpu.VMEM((n * span, across_q), f32),
            pltpu.VMEM((total + n * span, across_q), bf16),
            pltpu.VMEM((2, stack + 16, total + n * span), bf16),
            pltpu.VMEM((2, stack, across_q), f32),
            pltpu.VMEM((2, total, half * HEAD_DIM), bf16),
            pltpu.VMEM((2, total, half * HEAD_DIM), bf16),
            pltpu.VMEM((total, out_width), f32),
            pltpu.SemaphoreType.DMA((16,)),
            pltpu.SemaphoreType.DMA((n,)),
            pltpu.SemaphoreType.DMA((n,)),
            pltpu.SemaphoreType.DMA((n,)),
            pltpu.SemaphoreType.DMA((n,)),
            pltpu.SemaphoreType.DMA((blob_sends,)),
            pltpu.SemaphoreType.DMA((2, n)),
            pltpu.SemaphoreType.DMA((2, seqs)),
            pltpu.SemaphoreType.DMA((2, seqs)),
        ],
        compiler_params=pltpu.CompilerParams(
            collective_id=0, has_side_effects=True, vmem_limit_bytes=VMEM_BYTES
        ),
        name="layer",
    )(
        picks, hidden_in.reshape(total, width), w_sel_key, w_sel_value, w_cmp_key, w_cmp_value,
        key_out, value_out, cmp_key_in, cmp_value_in, w_query, gate_rows, lens, gain, w_out,
    )
    return out.reshape(seqs, span, out_width)


def fits(mesh):
    n = mesh.shape["kv"]
    return mesh.shape["tp"] == 2 and n % PLANE == 0 and n <= 32


def solution(mesh):
    placed = (
        P(None, "kv", None),
        P(None, "tp"),
        P(None, "tp"),
        P(None, "tp"),
        P(None, "tp"),
        P(None, "tp"),
        P(),
        P(),
        P(),
        P(),
        P(),
        P(),
        P(),
        P(),
        P(None, "kv", "tp", None),
    )
    return jax.shard_map(
        fused_shards if fits(mesh) else shards, mesh=mesh, in_specs=placed, out_specs=P(None, "kv", "tp"), check_vma=False
    )
```

time: 35.6 us -> 27.7 us (0.78)
  the two profiles are of different devices: /device:TPU:0 before, /device:TPU:19 now
where the time goes in v2:
time: 27.7 us; the launch traced here: 27.5 us
  Pallas kernels  26.7 us (96%)
  local copies, waits for them, and re-layouts  0.8 us (3%)
    pallas_call x1, Pallas kernels, fused_shards(): pl.pallas_call(functools.partial(layer_kernel, n, seqs, span, heads), in_...  26.7 us
    unnamed x1, local copies, waits for them, and re-layouts  0.8 us

profile of v2, /device:TPU:19, one launch (start us, length us, event | category | flops | bytes accessed | tf_op | source)
XLA Modules:
  0.0 27.5 jit_solution(16552308708224621479)
XLA Ops:
  0.0 26.7 %layer.1 = bf16[256,1024]{1,0:T(8,128)(2,1)S(1)} custom-call(s32[8,16]{1,0:T(8,128)} %bitcast.13, bf16[256,2048]{1,0:T(8,128)(2,1)} %bitcast.9, bf16[2048,128]{1,0:T(8,128)(2,1)} %wsk_ref.1, bf16[2048,128]{1,0:T(8,128)(2,1)} %wsv_ref.1, bf16[2048,128]{1,0:T(8,128)(2,1)} %wck_ref.1, bf16[2048,128]{1,0:T(8,128)(2,1)} %wcv_ref.1, bf16[64,128]{1,0:T(8,128)(2,1)} %bitcast.11, ...), custom_call_target="tpu_custom_call" | custom-call | tf_op jit(solution)/shard_map/layer/pallas_call | solution.py:747
  26.7 0.8 %copy.17 = bf16[4,64,1024]{2,1,0:T(8,128)(2,1)} copy(bf16[4,64,1024]{2,1,0:T(8,128)(2,1)S(1)} %bitcast.8) | data formatting | bytes 1048576

commit v3 on v2

--- a/solution.py
+++ b/solution.py
@@ -226,8 +226,8 @@
     wq_ref, wg_ref, lens_ref, gain_ref, wout_ref,
     out_ref,
     picks, rows, ws, kout, vout, kin, vin, wq, wg, lens, gain, weight,
-    qn, sk_buf, svt, raw, gate_buf, hits, lists, ents, blobs, near_s, far_s, probs, vals,
-    mix, own, other, partial,
+    qn, sk_buf, svt, raw, gate_buf, hits, lists, named_buf, ents, blobs, near_s, far_s, tops, base_top,
+    probs, base_sum, vals, mix, own, other, partial,
     load_sem, pick_send, pick_recv, ent_send, ent_recv, blob_send, blob_recv, half_send, half_recv,
 ):
     me = lax.axis_index("kv")
@@ -283,41 +283,54 @@
     cosine_e = jnp.cos(angle)
     sine_e = jnp.sin(angle) * sign[:entries]
 
+    near_keys = seqs * span
+    plane_keys = PLANE * span
+
+    def value_lanes(plane):
+        start = near_keys + (plane + planes - 1) % planes * plane_keys
+        return slice(start, start + plane_keys)
+
     for plane in range(1, planes):
         @pl.when(plane > z)
         def _():
+            for i in range(PLANE):
+                ents[plane * PLANE + i] = jnp.zeros((2 * entries, 128), bf16)
+            keys = slice(plane * plane_keys, (plane + 1) * plane_keys)
+            lanes = value_lanes(plane)
             for g in range(2):
-                for i in range(PLANE):
-                    blobs[g, plane * PLANE + i] = jnp.zeros((span, 128), bf16)
-
-    for d in range(1, n):
-        @pl.when(d > me)
-        def _():
-            ents[d] = jnp.zeros((2 * entries, 128), bf16)
+                far_s[g, keys, :] = jnp.zeros((plane_keys, across_q), f32)
+                vals[g, :, lanes] = jnp.zeros((stack + 16, plane_keys), bf16)
+                tops[g, plane * PLANE : (plane + 1) * PLANE] = jnp.zeros(
+                    (PLANE, 8, across_q), f32
+                )
 
     loads[0].wait()
+    pl.semaphore_wait(barrier, n)
+    sent = []
+
+    def send(src, dst, ssem, rsem, target, when=None):
+        copy = pltpu.make_async_remote_copy(
+            src_ref=src, dst_ref=dst, send_sem=ssem, recv_sem=rsem,
+            device_id=target, device_id_type=mesh_id,
+        )
+        if when is None:
+            copy.start()
+        else:
+            pl.when(when)(copy.start)
+        sent.append((copy, when))
+
+    for d in range(n - 1, 0, -1):
+        send(
+            picks, lists.at[me], pick_send.at[d - 1], pick_recv.at[me],
+            {"kv": (me + n - d) % n}, me >= d,
+        )
+
     slot_at = lax.broadcasted_iota(jnp.int32, (2 * seqs, TOPK), 1)
     listed = jnp.where(slot_at == 0, -1, picks[...])
     for b in range(n):
         hit = jnp.max(jnp.where(listed == b, 1.0, 0.0), axis=1, keepdims=True)
         hits[b] = jnp.broadcast_to(hit, (2 * seqs, 128))
-
-    pl.semaphore_wait(barrier, n)
-    sent = []
-
-    def send(src, dst, ssem, rsem, target, when=None):
-        copy = pltpu.make_async_remote_copy(
-            src_ref=src, dst_ref=dst, send_sem=ssem, recv_sem=rsem,
-            device_id=target, device_id_type=mesh_id,
-        )
-        if when is None:
-            copy.start()
-        else:
-            pl.when(when)(copy.start)
-        sent.append((copy, when))
-
-    for d in range(1, n):
-        send(picks, lists.at[me], pick_send.at[d - 1], pick_recv.at[me], {"kv": (me + d) % n})
+    named_buf[...] = jnp.zeros((2 * seqs, TOPK), f32)
 
     for load in loads[1:6]:
         load.wait()
@@ -356,11 +369,30 @@
         part = slice(g * entries, (g + 1) * entries)
         key = turn(results[0][part], cosine_e, sine_e)
         ents[me, part, :] = jnp.where(low_e, key, results[1][part]).astype(bf16)
-    for d in range(1, n):
-        send(
-            ents.at[me], ents.at[me], ent_send.at[d - 1], ent_recv.at[me],
-            {"kv": (me + d) % n}, me + d < n,
-        )
+    across = z * PLANE + (1 - x) * 2 + c
+    beside = z * PLANE + x * 2 + (1 - c)
+    side_slot = x * 2 + c
+    across_slot = (1 - x) * 2 + c
+    ent_number = [0]
+
+    def pass_entries(slot, dst, when=None):
+        ref = ents.at[slot]
+        send(ref, ref, ent_send.at[ent_number[0]], ent_recv.at[slot], {"kv": dst}, when)
+        ent_number[0] += 1
+
+    def entries_arrived(slot):
+        ref = ents.at[slot]
+        pltpu.make_async_remote_copy(
+            src_ref=ref, dst_ref=ref, send_sem=ent_send.at[0], recv_sem=ent_recv.at[slot],
+            device_id={"kv": (me + 1) % n}, device_id_type=mesh_id,
+        ).wait_recv()
+
+    for d in range(planes - 1, 0, -1):
+        up = jnp.minimum(z + d, planes - 1) * PLANE
+        pass_entries(me, up + side_slot, z + d < planes)
+        pass_entries(me, up + across_slot, z + d < planes)
+    pass_entries(me, across)
+    pass_entries(me, beside)
 
     for load in loads[10:14]:
         load.wait()
@@ -378,43 +410,16 @@
             lanes = slice(p * 128, (p + 1) * 128)
             qn[g, h * span : (h + 1) * span, lanes] = even.astype(bf16)
             qn[g, (h + 1) * span : (h + 2) * span, lanes] = odd.astype(bf16)
-    spread = 2 * wg_ref.shape[1]
-    logits = dot_t(wg[...].reshape(spread, rows.shape[1]), hidden)
-    wide_at = lax.broadcasted_iota(jnp.int32, (1, seqs * span), 1)
-    limit = jnp.zeros((1, seqs * span), jnp.int32)
-    for s in range(seqs):
-        limit = jnp.where(wide_at // span == s, lens[:, s : s + 1], limit)
-    live = me * span + wide_at % span < limit
-    for branch in range(2):
-        base = branch * (spread // 2)
-        mine = jnp.where(
-            column == 0, logits[base : base + heads], logits[base + heads : base + 2 * heads]
-        )
-        mine = jnp.where(live, jax.nn.sigmoid(mine), 0.0)
-        turned = [mine[:, p * 128 : (p + 1) * 128] for p in range(pairs)]
-        swapped = [swap(t) for t in turned]
-        for g in range(2):
-            for s in range(seqs):
-                for j in range(half // 2):
-                    one = slice(g * half + 2 * j, g * half + 2 * j + 1)
-                    two = slice(g * half + 2 * j + 1, g * half + 2 * j + 2)
-                    t, w = turned[s // 2], swapped[s // 2]
-                    if s % 2 == 0:
-                        row = jnp.where(low_row, t[one], w[two])
-                    else:
-                        row = jnp.where(low_row, w[one], t[two])
-                    number = (branch * 2 + g) * seqs + s
-                    gate_buf[number : number + 1, j * 128 : (j + 1) * 128] = row
-
-    named = jnp.zeros((2 * seqs, TOPK), f32)
-    for d in range(1, n):
-        origin = (me + d) % n
-        pltpu.make_async_remote_copy(
-            src_ref=picks, dst_ref=lists.at[origin], send_sem=pick_send.at[d - 1],
-            recv_sem=pick_recv.at[origin], device_id={"kv": origin}, device_id_type=mesh_id,
-        ).wait_recv()
-        named = jnp.where(lists[origin] == me, 1.0, named)
-    named = jnp.max(jnp.where(slot_at == 0, 0.0, named), axis=1, keepdims=True)
+    for b in range(1, n):
+        @pl.when(b > me)
+        def _():
+            pltpu.make_async_remote_copy(
+                src_ref=picks, dst_ref=lists.at[b], send_sem=pick_send.at[0],
+                recv_sem=pick_recv.at[b], device_id={"kv": (me + 1) % n}, device_id_type=mesh_id,
+            ).wait_recv()
+            named_buf[...] = jnp.where(lists[b] == me, 1.0, named_buf[...])
+
+    named = jnp.max(jnp.where(slot_at == 0, 0.0, named_buf[...]), axis=1, keepdims=True)
     named = jnp.broadcast_to(named, (2 * seqs, 128))
     key = jnp.zeros((span, 128), f32)
     for s in range(seqs):
@@ -444,39 +449,54 @@
             recv_sem=blob_recv.at[g, slot], device_id={"kv": (me + 1) % n}, device_id_type=mesh_id,
         ).wait_recv()
 
-    across = z * PLANE + (1 - x) * 2 + c
-    beside = z * PLANE + x * 2 + (1 - c)
-    side_slot = x * 2 + c
-    across_slot = (1 - x) * 2 + c
-    for g in range(2):
-        for d in range(planes - 1, 0, -1):
-            pass_on(g, me, me + d * PLANE, z + d < planes)
+    def export(g):
+        for d in range(1, planes):
+            up = jnp.minimum(z + d, planes - 1) * PLANE
+            pass_on(g, me, up + side_slot, z + d < planes)
+            pass_on(g, me, up + across_slot, z + d < planes)
         pass_on(g, me, across)
         pass_on(g, me, beside)
 
-    def from_below(g, d):
-        slot = jnp.maximum(z - d, 0) * PLANE + side_slot
-        pl.when(z >= d)(lambda: arrived(g, slot))
-        pass_on(g, slot, across, z >= d)
-        pass_on(g, slot, beside, z >= d)
-
-    def from_across(g, d):
-        slot = jnp.maximum(z - d, 0) * PLANE + across_slot
+    export(0)
+
+    def entries_direct(d):
+        base = jnp.maximum(z - d, 0) * PLANE
         if d == 0:
-            arrived(g, slot)
-            pass_on(g, slot, beside)
+            entries_arrived(across)
+            pass_entries(across, beside)
         else:
-            pl.when(z >= d)(lambda: arrived(g, slot))
-            pass_on(g, slot, beside, z >= d)
-
-    def from_beside(g):
-        for d in range(planes):
+            for slot in (base + side_slot, base + across_slot):
+                pl.when(z >= d)(functools.partial(entries_arrived, slot))
+                pass_entries(slot, beside, z >= d)
+
+    def entries_beside(d):
+        base = jnp.maximum(z - d, 0) * PLANE
+
+        def ready():
             for column_x in (x, 1 - x):
-                slot = jnp.maximum(z - d, 0) * PLANE + column_x * 2 + (1 - c)
-                if d == 0:
-                    arrived(g, slot)
-                else:
-                    pl.when(z >= d)(functools.partial(arrived, g, slot))
+                entries_arrived(base + column_x * 2 + (1 - c))
+
+        if d == 0:
+            ready()
+        else:
+            pl.when(z >= d)(ready)
+
+    def in_side(g, plane):
+        slot = plane * PLANE + side_slot
+        pl.when(z > plane)(lambda: arrived(g, slot))
+        pass_on(g, slot, beside, z > plane)
+
+    def in_cross(g, plane):
+        slot = plane * PLANE + across_slot
+        pl.when(z >= plane)(lambda: arrived(g, slot))
+        pass_on(g, slot, beside, z >= plane)
+
+    def plane_in(g, plane):
+        @pl.when(z >= plane)
+        def _():
+            for column_x in (x, 1 - x):
+                arrived(g, plane * PLANE + column_x * 2 + (1 - c))
+            plane_scores(g, plane)
 
     key_at = lax.broadcasted_iota(jnp.int32, (span, across_q), 0)
     query_at = lax.broadcasted_iota(jnp.int32, (span, across_q), 1) % span
@@ -484,8 +504,6 @@
     seq_lane = lax.broadcasted_iota(jnp.int32, (HEAD_DIM, seqs * span), 1) // span
     ones_at = lax.broadcasted_iota(jnp.int32, (16, seqs * span), 0)
     ones_lane = lax.broadcasted_iota(jnp.int32, (16, seqs * span), 1) // span
-    near_keys = seqs * span
-    near_top = {}
 
     def near_part(g):
         for s in range(seqs):
@@ -496,7 +514,7 @@
             lanes = slice((s // 2) * 128, (s // 2 + 1) * 128)
             score = dot_t(block, qn[g, :, lanes]) + near_bias
             near_s[g, s * span : (s + 1) * span, :] = score
-            near_top[g, s] = jnp.max(score.reshape(span // 8, 8, across_q), axis=0)
+            tops[g, n + s] = jnp.max(score.reshape(span // 8, 8, across_q), axis=0)
             value = svt[g * HEAD_DIM : (g + 1) * HEAD_DIM, :].astype(f32)
             vals[g, s * HEAD_DIM : (s + 1) * HEAD_DIM, 0:near_keys] = jnp.where(
                 seq_lane == s, value, 0.0
@@ -520,16 +538,6 @@
     total_row = lax.broadcasted_iota(jnp.int32, (16, slots), 0)
     total_lane = (lax.broadcasted_iota(jnp.int32, (16, slots), 1) % entries) // count
     group_row = lax.broadcasted_iota(jnp.int32, (entries, across_q), 0)
-
-    def wait_entries():
-        for b in range(n):
-            @pl.when(b < me)
-            def _():
-                pltpu.make_async_remote_copy(
-                    src_ref=ents.at[b], dst_ref=ents.at[b], send_sem=ent_send.at[0],
-                    recv_sem=ent_recv.at[b], device_id={"kv": (me + 1) % n},
-                    device_id_type=mesh_id,
-                ).wait_recv()
 
     def cmp_part(g):
         part = slice(g * entries, (g + 1) * entries)
@@ -562,68 +570,100 @@
             block = slice(s * HEAD_DIM, (s + 1) * HEAD_DIM)
             mix[g, block, :] = made[block] * factor
 
-    def far_part(g):
-        tops = []
-        for plane in range(planes):
-            left = []
-            for i in range(PLANE):
-                b = plane * PLANE + i
-                block = blobs[g, b].astype(f32)
-                turned = swap(block)
-                twice = jnp.where(low, block, turned)
-                tiles = []
-                for p in range(pairs):
-                    r0, r1 = 4 * p + g, 4 * p + 2 + g
-                    flag = jnp.where(low_row, hits[b, r0 : r0 + 1], hits[b, r1 : r1 + 1])
-                    tiles.append(twice * flag)
-                left.append(jnp.concatenate(tiles, axis=1))
-                if i % 2 == 0:
-                    before = turned
-                else:
-                    value = jnp.where(low, before, block)
-                    lanes = slice(near_keys + (b - 1) * span, near_keys + (b + 1) * span)
-                    for s in range(seqs):
-                        r = 2 * s + g
-                        flag = jnp.where(low_row, hits[b - 1, r : r + 1], hits[b, r : r + 1])
-                        vals[g, s * HEAD_DIM : (s + 1) * HEAD_DIM, lanes] = (value * flag).astype(
-                            bf16
-                        )
-                    flags = [
-                        jnp.where(low_row, hits[b - 1, r : r + 1], hits[b, r : r + 1])
-                        for r in range(g, 2 * seqs, 2)
-                    ]
-                    flags.append(jnp.zeros((16 - seqs, 128), f32))
-                    vals[g, stack : stack + 16, lanes] = jnp.concatenate(flags, axis=0).astype(bf16)
-            score = dot_t(jnp.concatenate(left, axis=0).astype(bf16), qn[g])
-            far_s[plane * PLANE * span : (plane + 1) * PLANE * span, :] = score
-            for i in range(PLANE):
-                block = score[i * span : (i + 1) * span].reshape(span // 8, 8, across_q)
-                tops.append(jnp.max(block, axis=0))
-        wide_hits = [jnp.concatenate([hits[b], hits[b]], axis=1) for b in range(n)]
-        refs = [jnp.full((1, across_q), 1e30, f32) for _ in range(n)]
+    def plane_scores(g, plane):
+        base = plane * PLANE
+        first_lane = value_lanes(plane).start
+        left = []
+        for i in range(PLANE):
+            block = blobs[g, base + i].astype(f32)
+            turned = swap(block)
+            twice = jnp.where(low, block, turned)
+            tiles = []
+            for p in range(pairs):
+                r0, r1 = 4 * p + g, 4 * p + 2 + g
+                flag = jnp.where(
+                    low_row, hits[base + i, r0 : r0 + 1], hits[base + i, r1 : r1 + 1]
+                )
+                tiles.append(twice * flag)
+            left.append(jnp.concatenate(tiles, axis=1))
+            if i % 2 == 0:
+                before = turned
+            else:
+                value = jnp.where(low, before, block)
+                lanes = slice(first_lane + (i - 1) * span, first_lane + (i + 1) * span)
+                flags = [
+                    jnp.where(low_row, hits[base + i - 1, r : r + 1], hits[base + i, r : r + 1])
+                    for r in range(g, 2 * seqs, 2)
+                ]
+                for s in range(seqs):
+                    vals[g, s * HEAD_DIM : (s + 1) * HEAD_DIM, lanes] = (value * flags[s]).astype(
+                        bf16
+                    )
+                flags.append(jnp.zeros((16 - seqs, 128), f32))
+                vals[g, stack : stack + 16, lanes] = jnp.concatenate(flags, axis=0).astype(bf16)
+        score = dot_t(jnp.concatenate(left, axis=0).astype(bf16), qn[g])
+        far_s[g, base * span : base * span + plane_keys, :] = score
+        for i in range(PLANE):
+            block = score[i * span : (i + 1) * span].reshape(span // 8, 8, across_q)
+            tops[g, base + i] = jnp.max(block, axis=0)
+
+    def flag_of(b):
+        return jnp.concatenate([hits[b], hits[b]], axis=1) > 0
+
+    def far_base(g):
+        blocks = range(PLANE, n)
+        refs = {b: jnp.full((1, across_q), 1e30, f32) for b in blocks}
+        flags = {b: flag_of(b) for b in blocks}
         for s in range(seqs):
             r = 2 * s + g
-            top = near_top[g, s]
-            for b in range(n):
-                top = jnp.maximum(top, jnp.where(wide_hits[b][r : r + 1] > 0, tops[b], FAR))
+            top = tops[g, n + s]
+            for b in blocks:
+                top = jnp.maximum(top, jnp.where(flags[b][r : r + 1], tops[g, b], FAR))
             top = jnp.max(top, axis=0, keepdims=True)
-            for b in range(n):
-                refs[b] = jnp.where(wide_hits[b][r : r + 1] > 0, top, refs[b])
+            base_top[g, s : s + 1, :] = top
+            for b in blocks:
+                refs[b] = jnp.where(flags[b][r : r + 1], top, refs[b])
             part = slice(s * span, (s + 1) * span)
             probs[part, :] = jnp.exp(near_s[g, part, :] - top).astype(bf16)
-        for b in range(n):
-            part = slice(b * span, (b + 1) * span)
-            block = jnp.exp(far_s[part, :] - refs[b]).astype(bf16)
-            probs[near_keys + b * span : near_keys + (b + 1) * span, :] = block
-        made = dot(vals[g], probs[...])
+        for b in blocks:
+            block = jnp.exp(far_s[g, b * span : (b + 1) * span, :] - refs[b]).astype(bf16)
+            start = near_keys + (b - PLANE) * span
+            probs[start : start + span, :] = block
+        known = n * span
+        base_sum[g] = dot(vals[g, :, :known], probs[...])
+
+    def far_part(g):
+        refs = [jnp.full((1, across_q), 1e30, f32) for _ in range(PLANE)]
+        flags = [flag_of(b) for b in range(PLANE)]
+        scales = []
+        for s in range(seqs):
+            r = 2 * s + g
+            top = jnp.where(flags[0][r : r + 1], tops[g, 0], FAR)
+            for b in range(1, PLANE):
+                top = jnp.maximum(top, jnp.where(flags[b][r : r + 1], tops[g, b], FAR))
+            before = base_top[g, s : s + 1, :]
+            top = jnp.maximum(jnp.max(top, axis=0, keepdims=True), before)
+            scales.append(jnp.exp(before - top))
+            for b in range(PLANE):
+                refs[b] = jnp.where(flags[b][r : r + 1], top, refs[b])
+        w = jnp.concatenate(
+            [
+                jnp.exp(far_s[g, b * span : (b + 1) * span, :] - refs[b]).astype(bf16)
+                for b in range(PLANE)
+            ],
+            axis=0,
+        )
+        made = dot(vals[g, :, n * span :], w)
         for p in range(pairs):
             tiles = []
             for s in (2 * p, 2 * p + 1):
                 row = (2 + g) * seqs + s
-                total = jnp.maximum(made[stack + s : stack + s + 1], 1.0)
+                line = slice(stack + s, stack + s + 1)
+                total = jnp.maximum(base_sum[g, line, :] * scales[s] + made[line], 1.0)
                 factor = gate_buf[row : row + 1, :] / total
                 block = slice(s * HEAD_DIM, (s + 1) * HEAD_DIM)
-                tiles.append(mix[g, block, :] + made[block] * factor)
+                old = base_sum[g, block, :] * (scales[s] * factor)
+                tiles.append(mix[g, block, :] + old + made[block] * factor)
             both = jnp.concatenate(tiles, axis=0)
             for j in range(half // 2):
                 lanes = slice(j * 128, (j + 1) * 128)
@@ -643,32 +683,69 @@
             recv_sem=half_recv.at[g, s], device_id={"tp": 1 - column}, device_id_type=mesh_id,
         )
 
+    spread = 2 * wg_ref.shape[1]
+    logits = dot_t(wg[...].reshape(spread, rows.shape[1]), hidden)
+    wide_at = lax.broadcasted_iota(jnp.int32, (1, seqs * span), 1)
+    limit = jnp.zeros((1, seqs * span), jnp.int32)
+    for s in range(seqs):
+        limit = jnp.where(wide_at // span == s, lens[:, s : s + 1], limit)
+    live = me * span + wide_at % span < limit
+    for branch in range(2):
+        base = branch * (spread // 2)
+        mine = jnp.where(
+            column == 0, logits[base : base + heads], logits[base + heads : base + 2 * heads]
+        )
+        mine = jnp.where(live, jax.nn.sigmoid(mine), 0.0)
+        turned = [mine[:, p * 128 : (p + 1) * 128] for p in range(pairs)]
+        swapped = [swap(t) for t in turned]
+        for g in range(2):
+            for s in range(seqs):
+                for j in range(half // 2):
+                    one = slice(g * half + 2 * j, g * half + 2 * j + 1)
+                    two = slice(g * half + 2 * j + 1, g * half + 2 * j + 2)
+                    t, w = turned[s // 2], swapped[s // 2]
+                    if s % 2 == 0:
+                        row = jnp.where(low_row, t[one], w[two])
+                    else:
+                        row = jnp.where(low_row, w[one], t[two])
+                    line = (branch * 2 + g) * seqs + s
+                    gate_buf[line : line + 1, j * 128 : (j + 1) * 128] = row
+
     for g in range(2):
         near_part(g)
-    from_across(0, 0)
-    if planes > 1:
-        from_below(0, 1)
-    from_across(1, 0)
-    for d in range(2, planes):
-        from_below(0, d)
-        from_below(1, d - 1)
-    wait_entries()
+    last = planes - 1
+    for plane in range(last - 1, 0, -1):
+        in_side(0, plane)
+        in_cross(0, plane + 1)
+    in_cross(0, 1)
+    export(1)
+    for d in range(planes):
+        entries_direct(d)
+    for plane in range(last, 1, -1):
+        plane_in(0, plane)
+    for d in range(planes):
+        entries_beside(d)
     cmp_part(0)
-    for d in range(1, planes):
-        from_across(0, d)
-        if d == planes - 2:
-            from_below(1, planes - 1)
-    for d in range(1, planes - 1):
-        from_across(1, d)
-    if planes == 2:
-        from_below(1, 1)
-    from_beside(0)
+    in_side(0, 0)
+    plane_in(0, 1)
+    in_cross(0, 0)
+    for plane in range(last - 1, 0, -1):
+        in_side(1, plane)
+    in_cross(1, last)
+    far_base(0)
+    plane_in(0, 0)
     far_part(0)
-    from_across(1, planes - 1)
+    for plane in range(last - 1, 0, -1):
+        in_cross(1, plane)
+    in_side(1, 0)
+    in_cross(1, 0)
     for load in loads[14:]:
         load.wait()
     cmp_part(1)
-    from_beside(1)
+    for plane in range(last, 0, -1):
+        plane_in(1, plane)
+    far_base(1)
+    plane_in(1, 0)
     far_part(1)
 
     squares = jnp.zeros((seqs * span, 1), f32)
@@ -743,7 +820,7 @@
     key_out, value_out = jnp.transpose(cmp_key_out), jnp.transpose(cmp_value_out)
     lens = seq_lengths[None]
     gain = out_gain[None]
-    blob_sends = 2 * (planes + 1) + 2 * (2 * (planes - 1) + planes)
+    blob_sends = 2 * (6 * planes)
     out = pl.pallas_call(
         functools.partial(layer_kernel, n, seqs, span, heads),
         in_specs=[anywhere] * 15,
@@ -769,11 +846,15 @@
             pltpu.VMEM((4 * seqs, across_q), f32),
             pltpu.VMEM((n, 2 * seqs, 128), f32),
             pltpu.VMEM((n,) + picks.shape, jnp.int32),
+            pltpu.VMEM(picks.shape, f32),
             pltpu.VMEM((n, 2 * entries, 128), bf16),
             pltpu.VMEM((2, n, span, 128), bf16),
             pltpu.VMEM((2, total, across_q), f32),
-            pltpu.VMEM((n * span, across_q), f32),
-            pltpu.VMEM((total + n * span, across_q), bf16),
+            pltpu.VMEM((2, n * span, across_q), f32),
+            pltpu.VMEM((2, n + seqs, 8, across_q), f32),
+            pltpu.VMEM((2, 8, across_q), f32),
+            pltpu.VMEM((n * span, across_q), bf16),
+            pltpu.VMEM((2, stack + 16, across_q), f32),
             pltpu.VMEM((2, stack + 16, total + n * span), bf16),
             pltpu.VMEM((2, stack, across_q), f32),
             pltpu.VMEM((2, total, half * HEAD_DIM), bf16),
@@ -782,7 +863,7 @@
             pltpu.SemaphoreType.DMA((16,)),
             pltpu.SemaphoreType.DMA((n,)),
             pltpu.SemaphoreType.DMA((n,)),
-            pltpu.SemaphoreType.DMA((n,)),
+            pltpu.SemaphoreType.DMA((4 * planes,)),
             pltpu.SemaphoreType.DMA((n,)),
             pltpu.SemaphoreType.DMA((blob_sends,)),
             pltpu.SemaphoreType.DMA((2, n)),
@@ -802,7 +883,7 @@
 
 def fits(mesh):
     n = mesh.shape["kv"]
-    return mesh.shape["tp"] == 2 and n % PLANE == 0 and n <= 32
+    return mesh.shape["tp"] == 2 and n % PLANE == 0 and 3 * PLANE <= n <= 32
 
 
 def solution(mesh):

time: 27.7 us -> 25.9 us (0.935)
  the two profiles are of different devices: /device:TPU:19 before, /device:TPU:24 now
where the time goes in v3:
time: 25.9 us; the launch traced here: 25.7 us
  Pallas kernels  24.9 us (96%)
  local copies, waits for them, and re-layouts  0.8 us (3%)
    pallas_call x1, Pallas kernels, fused_shards(): pl.pallas_call(functools.partial(layer_kernel, n, seqs, span, heads), in_...  24.9 us
    unnamed x1, local copies, waits for them, and re-layouts  0.8 us

profile of v3, /device:TPU:24, one launch (start us, length us, event | category | flops | bytes accessed | tf_op | source)
XLA Modules:
  0.0 25.7 jit_solution(7418419527926732769)
XLA Ops:
  0.0 24.9 %layer.1 = bf16[256,1024]{1,0:T(8,128)(2,1)S(1)} custom-call(s32[8,16]{1,0:T(8,128)} %bitcast.13, bf16[256,2048]{1,0:T(8,128)(2,1)} %bitcast.9, bf16[2048,128]{1,0:T(8,128)(2,1)} %wsk_ref.1, bf16[2048,128]{1,0:T(8,128)(2,1)} %wsv_ref.1, bf16[2048,128]{1,0:T(8,128)(2,1)} %wck_ref.1, bf16[2048,128]{1,0:T(8,128)(2,1)} %wcv_ref.1, bf16[64,128]{1,0:T(8,128)(2,1)} %bitcast.11, ...), custom_call_target="tpu_custom_call" | custom-call | tf_op jit(solution)/shard_map/layer/pallas_call | solution.py:824
  24.9 0.8 %copy.17 = bf16[4,64,1024]{2,1,0:T(8,128)(2,1)} copy(bf16[4,64,1024]{2,1,0:T(8,128)(2,1)S(1)} %bitcast.8) | data formatting | bytes 1048576

commit v4 on v3

--- a/solution.py
+++ b/solution.py
@@ -226,7 +226,7 @@
     wq_ref, wg_ref, lens_ref, gain_ref, wout_ref,
     out_ref,
     picks, rows, ws, kout, vout, kin, vin, wq, wg, lens, gain, weight,
-    qn, sk_buf, svt, raw, gate_buf, hits, lists, named_buf, ents, blobs, near_s, far_s, tops, base_top,
+    qn, sk_buf, svt, raw, gate_buf, hits, lists, ents, blobs, near_s, far_s, tops, base_top,
     probs, base_sum, vals, mix, own, other, partial,
     load_sem, pick_send, pick_recv, ent_send, ent_recv, blob_send, blob_recv, half_send, half_recv,
 ):
@@ -263,7 +263,8 @@
             pl.ds(pl.multiple_of(column * wide, wide), wide),
         ]
         jobs.append((block, weight.at[i]))
-    loads = [pltpu.make_async_copy(a, b, load_sem.at[i]) for i, (a, b) in enumerate(jobs)]
+    shared = [0, 1, 2, 2, 2, 2, 3, 4, 5, 6, 7, 8, 9, 10, 11, 11]
+    loads = [pltpu.make_async_copy(a, b, load_sem.at[i]) for i, (a, b) in zip(shared, jobs)]
     for load in loads:
         load.start()
 
@@ -306,8 +307,6 @@
 
     loads[0].wait()
     pl.semaphore_wait(barrier, n)
-    sent = []
-
     def send(src, dst, ssem, rsem, target, when=None):
         copy = pltpu.make_async_remote_copy(
             src_ref=src, dst_ref=dst, send_sem=ssem, recv_sem=rsem,
@@ -317,12 +316,18 @@
             copy.start()
         else:
             pl.when(when)(copy.start)
-        sent.append((copy, when))
 
     for d in range(n - 1, 0, -1):
         send(
-            picks, lists.at[me], pick_send.at[d - 1], pick_recv.at[me],
-            {"kv": (me + n - d) % n}, me >= d,
+            picks, lists.at[me], pick_send.at[0], pick_recv.at[0], {"kv": (me + n - d) % n},
+            me >= d,
+        )
+
+    def lists_copy(amount):
+        ref = lists.at[pl.ds(0, amount)]
+        return pltpu.make_async_remote_copy(
+            src_ref=ref, dst_ref=ref, send_sem=pick_send.at[0], recv_sem=pick_recv.at[0],
+            device_id={"kv": (me + 1) % n}, device_id_type=mesh_id,
         )
 
     slot_at = lax.broadcasted_iota(jnp.int32, (2 * seqs, TOPK), 1)
@@ -330,10 +335,9 @@
     for b in range(n):
         hit = jnp.max(jnp.where(listed == b, 1.0, 0.0), axis=1, keepdims=True)
         hits[b] = jnp.broadcast_to(hit, (2 * seqs, 128))
-    named_buf[...] = jnp.zeros((2 * seqs, TOPK), f32)
-
-    for load in loads[1:6]:
-        load.wait()
+
+    loads[1].wait()
+    pltpu.make_async_copy(ws, ws, load_sem.at[2]).wait()
     made = dot(rows[...], ws[...])
     sv = []
     for s in range(seqs):
@@ -373,12 +377,9 @@
     beside = z * PLANE + x * 2 + (1 - c)
     side_slot = x * 2 + c
     across_slot = (1 - x) * 2 + c
-    ent_number = [0]
-
     def pass_entries(slot, dst, when=None):
         ref = ents.at[slot]
-        send(ref, ref, ent_send.at[ent_number[0]], ent_recv.at[slot], {"kv": dst}, when)
-        ent_number[0] += 1
+        send(ref, ref, ent_send.at[0], ent_recv.at[slot], {"kv": dst}, when)
 
     def entries_arrived(slot):
         ref = ents.at[slot]
@@ -410,16 +411,12 @@
             lanes = slice(p * 128, (p + 1) * 128)
             qn[g, h * span : (h + 1) * span, lanes] = even.astype(bf16)
             qn[g, (h + 1) * span : (h + 2) * span, lanes] = odd.astype(bf16)
+    for b in range(n - 1):
+        pl.when(me == b)(lambda b=b: lists_copy(n - 1 - b).wait_recv())
+    named = jnp.zeros((2 * seqs, TOPK), f32)
     for b in range(1, n):
-        @pl.when(b > me)
-        def _():
-            pltpu.make_async_remote_copy(
-                src_ref=picks, dst_ref=lists.at[b], send_sem=pick_send.at[0],
-                recv_sem=pick_recv.at[b], device_id={"kv": (me + 1) % n}, device_id_type=mesh_id,
-            ).wait_recv()
-            named_buf[...] = jnp.where(lists[b] == me, 1.0, named_buf[...])
-
-    named = jnp.max(jnp.where(slot_at == 0, 0.0, named_buf[...]), axis=1, keepdims=True)
+        named = jnp.where((lists[b] == me) & (me < b), 1.0, named)
+    named = jnp.max(jnp.where(slot_at == 0, 0.0, named), axis=1, keepdims=True)
     named = jnp.broadcast_to(named, (2 * seqs, 128))
     key = jnp.zeros((span, 128), f32)
     for s in range(seqs):
@@ -435,12 +432,9 @@
         value = value + swap(value)
         blobs[g, me] = jnp.where(low, key if g == 0 else swap(key), value).astype(bf16)
 
-    number = [0]
-
     def pass_on(g, slot, dst, when=None):
         ref = blobs.at[g, slot]
-        send(ref, ref, blob_send.at[number[0]], blob_recv.at[g, slot], {"kv": dst}, when)
-        number[0] += 1
+        send(ref, ref, blob_send.at[0], blob_recv.at[g, slot], {"kv": dst}, when)
 
     def arrived(g, slot):
         ref = blobs.at[g, slot]
@@ -679,8 +673,8 @@
     def piece(g, s):
         part = pl.ds(s * span, span)
         return pltpu.make_async_remote_copy(
-            src_ref=own.at[g, part], dst_ref=other.at[g, part], send_sem=half_send.at[g, s],
-            recv_sem=half_recv.at[g, s], device_id={"tp": 1 - column}, device_id_type=mesh_id,
+            src_ref=own.at[g, part], dst_ref=other.at[g, part], send_sem=half_send.at[0],
+            recv_sem=half_recv.at[g * (s + 1)], device_id={"tp": 1 - column}, device_id_type=mesh_id,
         )
 
     spread = 2 * wg_ref.shape[1]
@@ -714,33 +708,35 @@
     for g in range(2):
         near_part(g)
     last = planes - 1
-    for plane in range(last - 1, 0, -1):
+    in_side(0, last - 1)
+    in_cross(0, last)
+    for d in range(planes):
+        entries_direct(d)
+    for plane in range(last - 2, 0, -1):
         in_side(0, plane)
         in_cross(0, plane + 1)
     in_cross(0, 1)
     export(1)
-    for d in range(planes):
-        entries_direct(d)
-    for plane in range(last, 1, -1):
-        plane_in(0, plane)
+    plane_in(0, last)
     for d in range(planes):
         entries_beside(d)
     cmp_part(0)
+    for plane in range(last - 1, 1, -1):
+        plane_in(0, plane)
     in_side(0, 0)
+    in_cross(0, 0)
     plane_in(0, 1)
-    in_cross(0, 0)
-    for plane in range(last - 1, 0, -1):
-        in_side(1, plane)
-    in_cross(1, last)
     far_base(0)
     plane_in(0, 0)
     far_part(0)
     for plane in range(last - 1, 0, -1):
+        in_side(1, plane)
+    in_cross(1, last)
+    for plane in range(last - 1, 0, -1):
         in_cross(1, plane)
     in_side(1, 0)
     in_cross(1, 0)
-    for load in loads[14:]:
-        load.wait()
+    pltpu.make_async_copy(weight, weight, load_sem.at[11]).wait()
     cmp_part(1)
     for plane in range(last, 0, -1):
         plane_in(1, plane)
@@ -760,8 +756,13 @@
         squares = squares + jnp.sum(a * a, axis=1, keepdims=True)
         scaled = (a * gains(column, g)).astype(bf16)
         total = total + dot(scaled, weight[0, g * group : (g + 1) * group, :])
-    for s in range(seqs):
-        piece(0, s).wait_recv()
+    def all_pieces(ref):
+        return pltpu.make_async_remote_copy(
+            src_ref=ref, dst_ref=ref, send_sem=half_send.at[0], recv_sem=half_recv.at[0],
+            device_id={"tp": 1 - column}, device_id_type=mesh_id,
+        )
+
+    all_pieces(other.at[0]).wait_recv()
     a = other[0].astype(f32)
     squares = squares + jnp.sum(a * a, axis=1, keepdims=True)
     scaled = (a * gains(1 - column, 0)).astype(bf16)
@@ -776,14 +777,18 @@
         done = partial[part, :] + dot(scaled, weight[1, group:, :])
         out_ref[part, :] = (done * row_scale).astype(bf16)
 
-    for g in range(2):
-        for s in range(seqs):
-            piece(g, s).wait_send()
-    for copy, when in sent:
-        if when is None:
-            copy.wait_send()
-        else:
-            pl.when(when)(copy.wait_send)
+    all_pieces(own).wait_send()
+    for b in range(1, n):
+        pl.when(me == b)(lambda b=b: lists_copy(b).wait_send())
+    everyone = pl.ds(0, 2 * planes + 1)
+    pltpu.make_async_remote_copy(
+        src_ref=ents.at[everyone], dst_ref=ents.at[everyone], send_sem=ent_send.at[0],
+        recv_sem=ent_recv.at[0], device_id={"kv": (me + 1) % n}, device_id_type=mesh_id,
+    ).wait_send()
+    pltpu.make_async_remote_copy(
+        src_ref=blobs.at[:, everyone], dst_ref=blobs.at[:, everyone], send_sem=blob_send.at[0],
+        recv_sem=blob_recv.at[0, 0], device_id={"kv": (me + 1) % n}, device_id_type=mesh_id,
+    ).wait_send()
 
 
 def fused_shards(
@@ -820,7 +825,6 @@
     key_out, value_out = jnp.transpose(cmp_key_out), jnp.transpose(cmp_value_out)
     lens = seq_lengths[None]
     gain = out_gain[None]
-    blob_sends = 2 * (6 * planes)
     out = pl.pallas_call(
         functools.partial(layer_kernel, n, seqs, span, heads),
         in_specs=[anywhere] * 15,
@@ -846,7 +850,6 @@
             pltpu.VMEM((4 * seqs, across_q), f32),
             pltpu.VMEM((n, 2 * seqs, 128), f32),
             pltpu.VMEM((n,) + picks.shape, jnp.int32),
-            pltpu.VMEM(picks.shape, f32),
             pltpu.VMEM((n, 2 * entries, 128), bf16),
             pltpu.VMEM((2, n, span, 128), bf16),
             pltpu.VMEM((2, total, across_q), f32),
@@ -860,15 +863,15 @@
             pltpu.VMEM((2, total, half * HEAD_DIM), bf16),
             pltpu.VMEM((2, total, half * HEAD_DIM), bf16),
             pltpu.VMEM((total, out_width), f32),
-            pltpu.SemaphoreType.DMA((16,)),
+            pltpu.SemaphoreType.DMA((12,)),
+            pltpu.SemaphoreType.DMA((1,)),
+            pltpu.SemaphoreType.DMA((1,)),
+            pltpu.SemaphoreType.DMA((1,)),
             pltpu.SemaphoreType.DMA((n,)),
-            pltpu.SemaphoreType.DMA((n,)),
-            pltpu.SemaphoreType.DMA((4 * planes,)),
-            pltpu.SemaphoreType.DMA((n,)),
-            pltpu.SemaphoreType.DMA((blob_sends,)),
+            pltpu.SemaphoreType.DMA((1,)),
             pltpu.SemaphoreType.DMA((2, n)),
-            pltpu.SemaphoreType.DMA((2, seqs)),
-            pltpu.SemaphoreType.DMA((2, seqs)),
+            pltpu.SemaphoreType.DMA((1,)),
+            pltpu.SemaphoreType.DMA((1 + seqs,)),
         ],
         compiler_params=pltpu.CompilerParams(
             collective_id=0, has_side_effects=True, vmem_limit_bytes=VMEM_BYTES

time: 25.9 us -> 24 us (0.927)
  Pallas kernels: 24.9 us -> 23.1 us
    pallas_call x1, Pallas kernels: 24.9 us -> 23.1 us  [fused_shards(): pl.pallas_call(functools.partial(layer_kernel, n, seqs, span, heads), in_...]
where the time goes in v4:
time: 24 us; the launch traced here: 23.9 us
  Pallas kernels  23.1 us (96%)
  local copies, waits for them, and re-layouts  0.8 us (3%)
    pallas_call x1, Pallas kernels, fused_shards(): pl.pallas_call(functools.partial(layer_kernel, n, seqs, span, heads), in_...  23.1 us
    unnamed x1, local copies, waits for them, and re-layouts  0.8 us

profile of v4, /device:TPU:24, one launch (start us, length us, event | category | flops | bytes accessed | tf_op | source)
XLA Modules:
  0.0 23.9 jit_solution(4863970482952105763)
XLA Ops:
  0.0 23.1 %layer.1 = bf16[256,1024]{1,0:T(8,128)(2,1)S(1)} custom-call(s32[8,16]{1,0:T(8,128)} %bitcast.13, bf16[256,2048]{1,0:T(8,128)(2,1)} %bitcast.9, bf16[2048,128]{1,0:T(8,128)(2,1)} %wsk_ref.1, bf16[2048,128]{1,0:T(8,128)(2,1)} %wsv_ref.1, bf16[2048,128]{1,0:T(8,128)(2,1)} %wck_ref.1, bf16[2048,128]{1,0:T(8,128)(2,1)} %wcv_ref.1, bf16[64,128]{1,0:T(8,128)(2,1)} %bitcast.11, ...), custom_call_target="tpu_custom_call" | custom-call | tf_op jit(solution)/shard_map/layer/pallas_call | solution.py:828
  23.1 0.8 %copy.17 = bf16[4,64,1024]{2,1,0:T(8,128)(2,1)} copy(bf16[4,64,1024]{2,1,0:T(8,128)(2,1)S(1)} %bitcast.8) | data formatting | bytes 1048576

commit v5 on v4

--- a/solution.py
+++ b/solution.py
@@ -377,23 +377,23 @@
     beside = z * PLANE + x * 2 + (1 - c)
     side_slot = x * 2 + c
     across_slot = (1 - x) * 2 + c
-    def pass_entries(slot, dst, when=None):
+    def pass_entries(slot, dst, kind, when=None):
         ref = ents.at[slot]
-        send(ref, ref, ent_send.at[0], ent_recv.at[slot], {"kv": dst}, when)
-
-    def entries_arrived(slot):
-        ref = ents.at[slot]
-        pltpu.make_async_remote_copy(
-            src_ref=ref, dst_ref=ref, send_sem=ent_send.at[0], recv_sem=ent_recv.at[slot],
+        send(ref, ref, ent_send.at[0], ent_recv.at[kind], {"kv": dst}, when)
+
+    def entries_copy(amount, kind):
+        ref = ents.at[pl.ds(0, amount)]
+        return pltpu.make_async_remote_copy(
+            src_ref=ref, dst_ref=ref, send_sem=ent_send.at[0], recv_sem=ent_recv.at[kind],
             device_id={"kv": (me + 1) % n}, device_id_type=mesh_id,
-        ).wait_recv()
+        )
 
     for d in range(planes - 1, 0, -1):
         up = jnp.minimum(z + d, planes - 1) * PLANE
-        pass_entries(me, up + side_slot, z + d < planes)
-        pass_entries(me, up + across_slot, z + d < planes)
-    pass_entries(me, across)
-    pass_entries(me, beside)
+        pass_entries(me, up + side_slot, 0, z + d < planes)
+        pass_entries(me, up + across_slot, 0, z + d < planes)
+    pass_entries(me, across, 0)
+    pass_entries(me, beside, 1)
 
     for load in loads[10:14]:
         load.wait()
@@ -432,64 +432,53 @@
         value = value + swap(value)
         blobs[g, me] = jnp.where(low, key if g == 0 else swap(key), value).astype(bf16)
 
-    def pass_on(g, slot, dst, when=None):
+    def pass_on(g, slot, dst, kind, when=None):
         ref = blobs.at[g, slot]
-        send(ref, ref, blob_send.at[0], blob_recv.at[g, slot], {"kv": dst}, when)
-
-    def arrived(g, slot):
-        ref = blobs.at[g, slot]
+        send(ref, ref, blob_send.at[0], blob_recv.at[g, slot // PLANE, kind], {"kv": dst}, when)
+
+    def arrived(g, plane, kind):
+        ref = blobs.at[g, pl.ds(0, 2)] if kind == 2 else blobs.at[g, 0]
         pltpu.make_async_remote_copy(
             src_ref=ref, dst_ref=ref, send_sem=blob_send.at[0],
-            recv_sem=blob_recv.at[g, slot], device_id={"kv": (me + 1) % n}, device_id_type=mesh_id,
+            recv_sem=blob_recv.at[g, plane, kind], device_id={"kv": (me + 1) % n},
+            device_id_type=mesh_id,
         ).wait_recv()
 
     def export(g):
         for d in range(1, planes):
             up = jnp.minimum(z + d, planes - 1) * PLANE
-            pass_on(g, me, up + side_slot, z + d < planes)
-            pass_on(g, me, up + across_slot, z + d < planes)
-        pass_on(g, me, across)
-        pass_on(g, me, beside)
+            pass_on(g, me, up + side_slot, 0, z + d < planes)
+            pass_on(g, me, up + across_slot, 1, z + d < planes)
+        pass_on(g, me, across, 1)
+        pass_on(g, me, beside, 2)
 
     export(0)
 
-    def entries_direct(d):
-        base = jnp.maximum(z - d, 0) * PLANE
-        if d == 0:
-            entries_arrived(across)
-            pass_entries(across, beside)
-        else:
-            for slot in (base + side_slot, base + across_slot):
-                pl.when(z >= d)(functools.partial(entries_arrived, slot))
-                pass_entries(slot, beside, z >= d)
-
-    def entries_beside(d):
-        base = jnp.maximum(z - d, 0) * PLANE
-
-        def ready():
-            for column_x in (x, 1 - x):
-                entries_arrived(base + column_x * 2 + (1 - c))
-
-        if d == 0:
-            ready()
-        else:
-            pl.when(z >= d)(ready)
+    def entries_direct():
+        for v in range(planes):
+            pl.when(z == v)(lambda v=v: entries_copy(2 * v + 1, 0).wait_recv())
+        for plane in range(planes):
+            pass_entries(plane * PLANE + side_slot, beside, 1, z > plane)
+            pass_entries(plane * PLANE + across_slot, beside, 1, z >= plane)
+
+    def entries_beside():
+        for v in range(planes):
+            pl.when(z == v)(lambda v=v: entries_copy(2 * v + 2, 1).wait_recv())
 
     def in_side(g, plane):
         slot = plane * PLANE + side_slot
-        pl.when(z > plane)(lambda: arrived(g, slot))
-        pass_on(g, slot, beside, z > plane)
+        pl.when(z > plane)(lambda: arrived(g, plane, 0))
+        pass_on(g, slot, beside, 2, z > plane)
 
     def in_cross(g, plane):
         slot = plane * PLANE + across_slot
-        pl.when(z >= plane)(lambda: arrived(g, slot))
-        pass_on(g, slot, beside, z >= plane)
+        pl.when(z >= plane)(lambda: arrived(g, plane, 1))
+        pass_on(g, slot, beside, 2, z >= plane)
 
     def plane_in(g, plane):
         @pl.when(z >= plane)
         def _():
-            for column_x in (x, 1 - x):
-                arrived(g, plane * PLANE + column_x * 2 + (1 - c))
+            arrived(g, plane, 2)
             plane_scores(g, plane)
 
     key_at = lax.broadcasted_iota(jnp.int32, (span, across_q), 0)
@@ -710,16 +699,14 @@
     last = planes - 1
     in_side(0, last - 1)
     in_cross(0, last)
-    for d in range(planes):
-        entries_direct(d)
+    entries_direct()
+    plane_in(0, last)
     for plane in range(last - 2, 0, -1):
         in_side(0, plane)
         in_cross(0, plane + 1)
     in_cross(0, 1)
     export(1)
-    plane_in(0, last)
-    for d in range(planes):
-        entries_beside(d)
+    entries_beside()
     cmp_part(0)
     for plane in range(last - 1, 1, -1):
         plane_in(0, plane)
@@ -762,6 +749,14 @@
             device_id={"tp": 1 - column}, device_id_type=mesh_id,
         )
 
+    for b in range(1, n):
+        pl.when(me == b)(lambda b=b: lists_copy(b).wait_send())
+    everyone = pl.ds(0, 2 * planes + 1)
+    entries_copy(2 * planes + 1, 0).wait_send()
+    pltpu.make_async_remote_copy(
+        src_ref=blobs.at[:, everyone], dst_ref=blobs.at[:, everyone], send_sem=blob_send.at[0],
+        recv_sem=blob_recv.at[0, 0, 0], device_id={"kv": (me + 1) % n}, device_id_type=mesh_id,
+    ).wait_send()
     all_pieces(other.at[0]).wait_recv()
     a = other[0].astype(f32)
     squares = squares + jnp.sum(a * a, axis=1, keepdims=True)
@@ -778,17 +773,6 @@
         out_ref[part, :] = (done * row_scale).astype(bf16)
 
     all_pieces(own).wait_send()
-    for b in range(1, n):
-        pl.when(me == b)(lambda b=b: lists_copy(b).wait_send())
-    everyone = pl.ds(0, 2 * planes + 1)
-    pltpu.make_async_remote_copy(
-        src_ref=ents.at[everyone], dst_ref=ents.at[everyone], send_sem=ent_send.at[0],
-        recv_sem=ent_recv.at[0], device_id={"kv": (me + 1) % n}, device_id_type=mesh_id,
-    ).wait_send()
-    pltpu.make_async_remote_copy(
-        src_ref=blobs.at[:, everyone], dst_ref=blobs.at[:, everyone], send_sem=blob_send.at[0],
-        recv_sem=blob_recv.at[0, 0], device_id={"kv": (me + 1) % n}, device_id_type=mesh_id,
-    ).wait_send()
 
 
 def fused_shards(
@@ -867,9 +851,9 @@
             pltpu.SemaphoreType.DMA((1,)),
             pltpu.SemaphoreType.DMA((1,)),
             pltpu.SemaphoreType.DMA((1,)),
-            pltpu.SemaphoreType.DMA((n,)),
+            pltpu.SemaphoreType.DMA((2,)),
             pltpu.SemaphoreType.DMA((1,)),
-            pltpu.SemaphoreType.DMA((2, n)),
+            pltpu.SemaphoreType.DMA((2, planes, 3)),
             pltpu.SemaphoreType.DMA((1,)),
             pltpu.SemaphoreType.DMA((1 + seqs,)),
         ],

time: 24 us -> 23.8 us (level)
  Pallas kernels: 23.1 us -> 22.8 us
where the time goes in v5:
time: 23.8 us; the launch traced here: 23.6 us
  Pallas kernels  22.8 us (96%)
  local copies, waits for them, and re-layouts  0.8 us (3%)
    pallas_call x1, Pallas kernels, fused_shards(): pl.pallas_call(functools.partial(layer_kernel, n, seqs, span, heads), in_...  22.8 us
    unnamed x1, local copies, waits for them, and re-layouts  0.8 us

profile of v5, /device:TPU:24, one launch (start us, length us, event | category | flops | bytes accessed | tf_op | source)
XLA Modules:
  0.0 23.6 jit_solution(13875415493468025599)
XLA Ops:
  0.0 22.8 %layer.1 = bf16[256,1024]{1,0:T(8,128)(2,1)S(1)} custom-call(s32[8,16]{1,0:T(8,128)} %bitcast.13, bf16[256,2048]{1,0:T(8,128)(2,1)} %bitcast.9, bf16[2048,128]{1,0:T(8,128)(2,1)} %wsk_ref.1, bf16[2048,128]{1,0:T(8,128)(2,1)} %wsv_ref.1, bf16[2048,128]{1,0:T(8,128)(2,1)} %wck_ref.1, bf16[2048,128]{1,0:T(8,128)(2,1)} %wcv_ref.1, bf16[64,128]{1,0:T(8,128)(2,1)} %bitcast.11, ...), custom_call_target="tpu_custom_call" | custom-call | tf_op jit(solution)/shard_map/layer/pallas_call | solution.py:812
  22.8 0.8 %copy.17 = bf16[4,64,1024]{2,1,0:T(8,128)(2,1)} copy(bf16[4,64,1024]{2,1,0:T(8,128)(2,1)S(1)} %bitcast.8) | data formatting | bytes 1048576

commit v6 on v5

--- a/solution.py
+++ b/solution.py
@@ -636,17 +636,20 @@
             ],
             axis=0,
         )
-        made = dot(vals[g, :, n * span :], w)
+        sums = dot(vals[g, stack:, n * span :], w)
         for p in range(pairs):
             tiles = []
+            made = dot(vals[g, p * 128 : (p + 1) * 128, n * span :], w)
             for s in (2 * p, 2 * p + 1):
                 row = (2 + g) * seqs + s
                 line = slice(stack + s, stack + s + 1)
-                total = jnp.maximum(base_sum[g, line, :] * scales[s] + made[line], 1.0)
+                total = base_sum[g, line, :] * scales[s] + sums[s : s + 1]
+                total = jnp.maximum(total, 1.0)
                 factor = gate_buf[row : row + 1, :] / total
                 block = slice(s * HEAD_DIM, (s + 1) * HEAD_DIM)
                 old = base_sum[g, block, :] * (scales[s] * factor)
-                tiles.append(mix[g, block, :] + old + made[block] * factor)
+                fresh = made[(s % 2) * HEAD_DIM : (s % 2 + 1) * HEAD_DIM]
+                tiles.append(mix[g, block, :] + old + fresh * factor)
             both = jnp.concatenate(tiles, axis=0)
             for j in range(half // 2):
                 lanes = slice(j * 128, (j + 1) * 128)

time: 23.8 us -> 23.8 us (level)
  no operation moved by 1% of the time
where the time goes in v6:
time: 23.8 us; the launch traced here: 23.6 us
  Pallas kernels  22.8 us (96%)
  local copies, waits for them, and re-layouts  0.8 us (3%)
    pallas_call x1, Pallas kernels, fused_shards(): pl.pallas_call(functools.partial(layer_kernel, n, seqs, span, heads), in_...  22.8 us
    unnamed x1, local copies, waits for them, and re-layouts  0.8 us

profile of v6, /device:TPU:24, one launch (start us, length us, event | category | flops | bytes accessed | tf_op | source)
XLA Modules:
  0.0 23.6 jit_solution(14721978184717060003)
XLA Ops:
  0.0 22.8 %layer.1 = bf16[256,1024]{1,0:T(8,128)(2,1)S(1)} custom-call(s32[8,16]{1,0:T(8,128)} %bitcast.13, bf16[256,2048]{1,0:T(8,128)(2,1)} %bitcast.9, bf16[2048,128]{1,0:T(8,128)(2,1)} %wsk_ref.1, bf16[2048,128]{1,0:T(8,128)(2,1)} %wsv_ref.1, bf16[2048,128]{1,0:T(8,128)(2,1)} %wck_ref.1, bf16[2048,128]{1,0:T(8,128)(2,1)} %wcv_ref.1, bf16[64,128]{1,0:T(8,128)(2,1)} %bitcast.11, ...), custom_call_target="tpu_custom_call" | custom-call | tf_op jit(solution)/shard_map/layer/pallas_call | solution.py:815
  22.8 0.8 %copy.17 = bf16[4,64,1024]{2,1,0:T(8,128)(2,1)} copy(bf16[4,64,1024]{2,1,0:T(8,128)(2,1)S(1)} %bitcast.8) | data formatting | bytes 1048576
